TPU v7x, 128 devices: a whole 4x4x4 slice. The times are simulated.
128 devices in a mesh: fs: 16 (over z, x), tp: 8 (over y, core).
Axes of the slice: x: 4, y: 4, z: 4, core: 2. Of those that a mesh axis runs over, the one named last changes fastest.
Arguments:
- inputs: bfloat16 [16384, 4096], P('fs'), may hold values from -8 to 8
- value_cot: bfloat16 [16384, 2048], P('fs', 'tp'), may hold values from -0.01171875 to 0.01171875
- gate_cot: bfloat16 [16384, 2048], P('fs', 'tp'), may hold values from -0.01171875 to 0.01171875
- out_cot: bfloat16 [16384, 4096], P('fs'), may hold values from -0.015625 to 0.015625
- conv_output: bfloat16 [16384, 2048], P('fs', 'tp'), may hold values from -6 to 6
- factors: bfloat16 [3, 4096, 256], P(None, 'fs'), may hold values from -0.375 to 0.375
- value_weight: float32 [4096, 2048], P('fs', 'tp'), may hold values from -0.09375 to 0.09375
- gate_weight: float32 [4096, 2048], P('fs', 'tp'), may hold values from -0.09375 to 0.09375
- out_weight: float32 [2048, 4096], P('tp', 'fs'), may hold values from -0.125 to 0.125
- first_moment: float32 [3, 256, 2048], P(None, 'fs', 'tp'), may hold values from -7.2 to 7.2
- second_moment: float32 [3, 256, 2048], P(None, 'fs', 'tp'), may hold values from 0.005 to 0.05
Outputs:
- new_first: float32 [3, 256, 2048], P(None, 'fs', 'tp')
- new_second: float32 [3, 256, 2048], P(None, 'fs', 'tp')
- value_update: float32 [4096, 2048], P('fs', 'tp')
- gate_update: float32 [4096, 2048], P('fs', 'tp')
- out_update: float32 [2048, 4096], P('tp', 'fs')
- value_copy: bfloat16 [4096, 2048], P(None, 'tp')
- gate_copy: bfloat16 [4096, 2048], P(None, 'tp')
- out_copy: bfloat16 [2048, 4096], P('tp')
All inputs are finite; a program needn't handle non-finite values.
Results may differ from a plain program's by a relative error of at most 0.001.
Values may be sent and summed in bfloat16 or wider, within the bound.
A program may use at most 128 MiB of HBM per device.

v0:
```python
import jax
import jax.numpy as jnp
from jax import lax
from jax.sharding import PartitionSpec as P

C = 2048
RANK = 256


FIRST_DECAY = 0.9
SECOND_DECAY = 0.95
DIVISOR_EPS = 1e-08
SQUARE_EPS = 1e-06
LEARN_RATE = 0.01


def in_blocks(array, dim, length):
    dims = array.shape
    pieces = array.reshape(*dims[:dim], length, dims[dim] // length, *dims[dim + 1 :])
    return jnp.moveaxis(pieces, dim, 0)


def sum_at_owner(array, axis, dim):
    pieces = in_blocks(array, dim, lax.axis_size(axis))
    arrived = lax.all_to_all(pieces, axis, split_axis=0, concat_axis=0, tiled=True)
    return arrived.sum(axis=0)


def from_everyone(array, axis):
    copies = jnp.broadcast_to(array, (lax.axis_size(axis), *array.shape))
    return lax.all_to_all(copies, axis, split_axis=0, concat_axis=0, tiled=True)


def laid_out(pieces, dim):
    pieces = jnp.moveaxis(pieces, 0, dim)
    dims = pieces.shape
    return pieces.reshape(*dims[:dim], dims[dim] * dims[dim + 1], *dims[dim + 2 :])


def gather_directly(array, axis, dim):
    pieces = from_everyone(array, axis)
    return laid_out(pieces, dim)


def over_copies(array, axis):
    everything = from_everyone(array, axis)
    return jnp.sum(everything, axis=0)


def rows_first(arrays, axis, dims):
    turned = [jnp.moveaxis(a, dim, 0) for a, dim in zip(arrays, dims)]
    both = jnp.concatenate([t.reshape(len(t), -1) for t in turned], axis=1)
    whole, at, gathered = (lax.all_gather(both, axis, axis=0, tiled=True), 0, [])
    for t, dim in zip(turned, dims):
        share = whole[:, at : at + t[0].size].reshape(-1, *t.shape[1:])
        gathered.append(jnp.moveaxis(share, 0, dim))
        at += t[0].size
    return tuple(gathered)


def high_low(values):
    upper = lax.optimization_barrier(values.astype(jnp.bfloat16))
    lower = (values - upper.astype(jnp.float32)).astype(jnp.bfloat16)
    return (upper, lower)


def split_product(left, right, transposed):
    upper, lower = high_low(right)
    operand = left.T if transposed else left
    first_part = jnp.dot(operand, upper, preferred_element_type=jnp.float32)
    return first_part + jnp.dot(operand, lower, preferred_element_type=jnp.float32)


def shards(
    inputs,
    value_cot,
    gate_cot,
    out_cot,
    conv_output,
    factors,
    value_weight,
    gate_weight,
    out_weight,
    first_moment,
    second_moment,
):
    col_width = value_cot.shape[1]
    rows_small = first_moment.shape[1]
    pieces = lax.all_gather(factors, "fs", axis=1, tiled=True)
    summed = jnp.stack(
        [
            jnp.dot(inputs, pieces[0], preferred_element_type=jnp.float32),
            jnp.dot(inputs, pieces[1], preferred_element_type=jnp.float32),
            jnp.dot(out_cot, pieces[2], preferred_element_type=jnp.float32),
        ]
    )
    partial_value = jnp.concatenate(
        [
            split_product(value_cot, summed[0], True).T,
            split_product(gate_cot, summed[1], True).T,
            split_product(conv_output, summed[2], True).T,
        ],
        axis=1,
    )
    projected = sum_at_owner(partial_value, "fs", 0)
    first_cols = jnp.transpose(first_moment, (1, 0, 2)).reshape(rows_small, 3 * col_width)
    second_cols = jnp.transpose(second_moment, (1, 0, 2)).reshape(rows_small, 3 * col_width)
    new_first = FIRST_DECAY * first_cols + (1.0 - FIRST_DECAY) * projected
    new_second = SECOND_DECAY * second_cols + (1.0 - SECOND_DECAY) * projected * projected
    direction = new_first / (jnp.sqrt(new_second) + DIVISOR_EPS)
    collected = gather_directly(direction, "fs", 0)
    sum_squares = over_copies(jnp.sum(collected * collected), "tp")
    norm_scale = lax.rsqrt(sum_squares / (3 * RANK * C) + SQUARE_EPS)
    updates = [
        norm_scale
        * split_product(
            factors[index], collected[:, index * col_width : (index + 1) * col_width], False
        )
        for index in range(3)
    ]
    out_update = updates[2].T
    copies = rows_first(
        (
            (value_weight - LEARN_RATE * updates[0]).astype(jnp.bfloat16),
            (gate_weight - LEARN_RATE * updates[1]).astype(jnp.bfloat16),
            (out_weight - LEARN_RATE * out_update).astype(jnp.bfloat16),
        ),
        "fs",
        (0, 0, 1),
    )
    first_out = jnp.transpose(new_first.reshape(rows_small, 3, col_width), (1, 0, 2))
    second_out = jnp.transpose(new_second.reshape(rows_small, 3, col_width), (1, 0, 2))
    return (
        first_out,
        second_out,
        updates[0],
        updates[1],
        out_update,
        copies[0],
        copies[1],
        copies[2],
    )


def solution(mesh):
    placed = (
        P("fs", None),
        P("fs", "tp"),
        P("fs", "tp"),
        P("fs", None),
        P("fs", "tp"),
        P(None, "fs", None),
        P("fs", "tp"),
        P("fs", "tp"),
        P("tp", "fs"),
        P(None, "fs", "tp"),
        P(None, "fs", "tp"),
    )
    return jax.shard_map(
        shards,
        mesh=mesh,
        in_specs=placed,
        out_specs=(
            P(None, "fs", "tp"),
            P(None, "fs", "tp"),
            P("fs", "tp"),
            P("fs", "tp"),
            P("tp", "fs"),
            P(None, "tp"),
            P(None, "tp"),
            P("tp", None),
        ),
        check_vma=False,
    )
```

profile of v0, /device:TPU:0, one launch (start us, length us, event | category | flops | bytes accessed | tf_op | source)
XLA Modules:
  0.0 229.1 jit_solution(9005867592654134200)
XLA Ops:
  7.2 0.0 copy-start
  7.2 0.0 all-gather.3.cloned.1.call-start
  7.2 0.7 all-gather.3.cloned.1.call-update
  7.9 66.2 %all-gather.3.cloned.1.call-done = bf16[3,4096,256]{2,1,0:T(8,128)(2,1)} async-done(((bf16[3,256,256]{2,1,0:T(8,128)(2,1)}), bf16[3,4096,256]{2,1,0:T(8,128)(2,1)}) %all-gather.3.cloned.1.call-update) | async-done | bytes 6291472 | tf_op jit(solution)/shard_map/all_gather | solution.py:89
  74.1 0.0 slice-start
  74.1 6.5 %fusion.35 = (bf16[1024,256]{1,0:T(8,128)(2,1)S(1)}, f32[1024,256]{1,0:T(8,128)S(1)}) fusion(bf16[1024,4096]{1,0:T(8,128)(2,1)} %param.11, bf16[3,4096,256]{2,1,0:T(8,128)(2,1)} %all-gather.3.cloned.1.call-done), kind=kOutput, calls=%fused_computation.65 | convolution fusion | flops 2147745792 | bytes 12058624 | tf_op jit(solution)/shard_map/dot_general | solution.py:92
  80.5 0.0 copy-done.8
  80.6 0.0 slice-start.1
  80.6 4.1 %fusion.34 = (bf16[1024,256]{1,0:T(8,128)(2,1)S(1)}, f32[1024,256]{1,0:T(8,128)S(1)}) fusion(bf16[1024,4096]{1,0:T(8,128)(2,1)S(1)} %copy-done.8, bf16[3,4096,256]{2,1,0:T(8,128)(2,1)} %all-gather.3.cloned.1.call-done), kind=kOutput, calls=%fused_computation.64 | convolution fusion | flops 2147745792 | bytes 12058624 | tf_op jit(solution)/shard_map/dot_general | solution.py:93
  84.6 0.0 slice-done
  84.7 0.0 slice-done.1
  84.7 0.0 copy-start.2
  84.7 4.0 %fusion.33 = (bf16[1024,256]{1,0:T(8,128)(2,1)S(1)}, f32[1024,256]{1,0:T(8,128)S(1)}) fusion(bf16[1024,4096]{1,0:T(8,128)(2,1)S(1)} %bitcast.89, bf16[3,4096,256]{2,1,0:T(8,128)(2,1)} %all-gather.3.cloned.1.call-done), kind=kOutput, calls=%fused_computation.63 | convolution fusion | flops 2147745792 | bytes 12058624 | tf_op jit(solution)/shard_map/dot_general | solution.py:94
  88.7 0.0 copy-start.3
  88.7 0.0 copy-done
  88.7 0.3 fusion.36
  89.0 0.4 convolution_add_fusion.5
  89.4 0.0 copy-done.2
  89.4 0.0 copy-start.7
  89.4 0.0 copy-start.6
  89.4 0.4 fusion.37
  89.8 0.4 convolution_add_fusion.4
  90.2 0.0 copy-done.3
  90.2 0.0 copy-start.5
  90.2 0.4 fusion.38
  90.5 0.0 copy-start.1
  90.5 0.4 convolution_add_fusion.3
  90.9 0.1 pad_maximum_fusion
  91.0 1.1 copy.87
  92.1 5.3 %all-to-all-start = ((f32[16,16,768]{2,1,0:T(8,128)}), f32[16,16,768]{2,1,0:T(8,128)S(1)}, u32[]{:S(2)}, u32[]{:S(2)}) async-start(f32[16,16,768]{2,1,0:T(8,128)} %bitcast.4), calls=%async_computation | async-start | bytes 1572864 | tf_op jit(solution)/shard_map/all_to_all | solution.py:25
  97.4 0.0 copy-done.7
  97.4 0.0 copy-done.6
  97.5 14.2 %all-to-all-done = f32[16,16,768]{2,1,0:T(8,128)S(1)} async-done(((f32[16,16,768]{2,1,0:T(8,128)}), f32[16,16,768]{2,1,0:T(8,128)S(1)}, u32[]{:S(2)}, u32[]{:S(2)}) %all-to-all-start) | async-done | bytes 786464 | tf_op jit(solution)/shard_map/all_to_all | solution.py:25
  111.8 1.0 broadcast_in_dim.6
  112.8 3.6 %all-to-all-start.1 = ((f32[16,16,768]{2,1,0:T(8,128)}), f32[16,16,768]{2,1,0:T(8,128)S(1)}, u32[]{:S(2)}, u32[]{:S(2)}) async-start(f32[16,16,768]{2,1,0:T(8,128)} %broadcast_in_dim.6), calls=%async_computation.1 | async-start | bytes 1572864 | tf_op jit(solution)/shard_map/all_to_all | solution.py:31
  116.4 0.0 copy-done.5
  116.4 0.1 copy.100
  116.5 13.2 %all-to-all-done.1 = f32[16,16,768]{2,1,0:T(8,128)S(1)} async-done(((f32[16,16,768]{2,1,0:T(8,128)}), f32[16,16,768]{2,1,0:T(8,128)S(1)}, u32[]{:S(2)}, u32[]{:S(2)}) %all-to-all-start.1) | async-done | bytes 786464 | tf_op jit(solution)/shard_map/all_to_all | solution.py:31
  129.8 0.0 copy-done.1
  129.8 0.2 fusion.9
  130.0 0.8 multiply_reduce_fusion
  130.8 1.2 broadcast_in_dim.7
  132.0 4.3 %all-to-all-start.2 = ((f32[8,1,1]{2,1,0:T(1,128)}), f32[8,1,1]{2,1,0:T(1,128)S(1)}, u32[]{:S(2)}, u32[]{:S(2)}) async-start(f32[8,1,1]{2,1,0:T(1,128)} %broadcast_in_dim.7), calls=%async_computation.2 | async-start | bytes 8192 | tf_op jit(solution)/shard_map/all_to_all | solution.py:31
  136.3 0.0 all-gather.5.cloned.1.call-start
  136.4 0.2 fusion.12
  136.6 0.2 fusion.16
  136.8 4.8 %all-to-all-done.2 = f32[8,1,1]{2,1,0:T(1,128)S(1)} async-done(((f32[8,1,1]{2,1,0:T(1,128)}), f32[8,1,1]{2,1,0:T(1,128)S(1)}, u32[]{:S(2)}, u32[]{:S(2)}) %all-to-all-start.2) | async-done | bytes 64 | tf_op jit(solution)/shard_map/all_to_all | solution.py:31
  141.5 0.6 reduce_sum.32
  142.9 0.2 fusion.3
  143.1 0.1 copy.104
  143.2 0.0 copy-start.4
  143.2 2.0 subtract_convert_fusion.7
  145.2 0.1 copy.102
  145.3 1.0 fusion.8
  146.3 0.2 subtract_convert_fusion.8
  146.5 0.8 pad_maximum_fusion.1
  147.3 0.0 all-gather.5.cloned.1.call-update
  147.3 0.7 fusion.25
  147.9 0.8 copy.103
  148.8 61.5 %all-gather.5.cloned.1.call-done = bf16[4096,768]{0,1:T(8,128)(2,1)} async-done(((bf16[256,768]{0,1:T(8,128)(2,1)}), bf16[4096,768]{0,1:T(8,128)(2,1)}) %all-gather.5.cloned.1.call-update) | async-done | bytes 6291472 | tf_op jit(solution)/shard_map/all_gather | solution.py:53
  210.3 5.5 %slice_bitcast_fusion = (bf16[256,4096]{1,0:T(8,128)(2,1)}, bf16[4096,256]{0,1:T(8,128)(2,1)S(1)}, bf16[4096,256]{0,1:T(8,128)(2,1)}) fusion(bf16[4096,768]{0,1:T(8,128)(2,1)} %all-gather.5.cloned.1.call-done), kind=kLoop, calls=%fused_computation | loop fusion | bytes 12582912 | tf_op jit(solution)/shard_map/transpose | solution.py:56
  215.8 0.0 copy-done.4
  215.8 4.1 %copy.105 = bf16[4096,256]{1,0:T(8,128)(2,1)} copy(bf16[4096,256]{0,1:T(8,128)(2,1)} %get-tuple-element.50) | data formatting | bytes 4194304
  219.9 2.4 %copy.106 = bf16[4096,256]{1,0:T(8,128)(2,1)} copy(bf16[4096,256]{0,1:T(8,128)(2,1)S(1)} %get-tuple-element.49) | data formatting | bytes 4194304
  (9 shorter events, 0.1 us)
Async XLA Ops:
  7.2 81.5 %copy-start = (bf16[1024,256]{1,0:T(8,128)(2,1)S(1)}, bf16[1024,256]{1,0:T(8,128)(2,1)}, u32[]{:S(2)}) copy-start(bf16[1024,256]{1,0:T(8,128)(2,1)} %param.12) | copy-start | bytes 1572868
  7.2 66.9 %all-gather.3.cloned.1.call-start = ((), (), s32[]{:S(2)}) async-start(), calls=%async_computation.3 | async-start | bytes 6684672 | tf_op jit(solution)/shard_map/all_gather | solution.py:89
  74.1 6.5 %copy-start.8 = (bf16[1024,4096]{1,0:T(8,128)(2,1)S(1)}, bf16[1024,4096]{1,0:T(8,128)(2,1)}, u32[]{:S(2)}) copy-start(bf16[1024,4096]{1,0:T(8,128)(2,1)} %param.11) | copy-start | bytes 25165828
  74.1 10.6 %slice-start = ((s8[8388608]{0:T(1024)(128)(4,1)}), s8[4194304]{0:T(1024)(128)(4,1)S(1)}, s32[]{:S(2)}) async-start(s8[8388608]{0:T(1024)(128)(4,1)} %bitcast.88), calls=%async_computation.5 | async-start | bytes 8388608
  80.6 4.1 %slice-start.1 = ((s8[8388608]{0:T(1024)(128)(4,1)}), s8[4194304]{0:T(1024)(128)(4,1)S(1)}, s32[]{:S(2)}) async-start(s8[8388608]{0:T(1024)(128)(4,1)} %bitcast.88), calls=%async_computation.6 | async-start | bytes 8388608
  84.7 4.7 %copy-start.2 = (bf16[1024,256]{1,0:T(8,128)(2,1)S(1)}, bf16[1024,256]{1,0:T(8,128)(2,1)}, u32[]{:S(2)}) copy-start(bf16[1024,256]{1,0:T(8,128)(2,1)} %param.13) | copy-start | bytes 1572868
  88.7 1.5 copy-start.3
  89.4 8.0 %copy-start.7 = (f32[3,16,256]{2,1,0:T(8,128)S(1)}, f32[3,16,256]{2,1,0:T(8,128)}, u32[]{:S(2)}) copy-start(f32[3,16,256]{2,1,0:T(8,128)} %param.20) | copy-start | bytes 147460
  89.4 8.0 %copy-start.6 = (f32[3,16,256]{2,1,0:T(8,128)S(1)}, f32[3,16,256]{2,1,0:T(8,128)}, u32[]{:S(2)}) copy-start(f32[3,16,256]{2,1,0:T(8,128)} %param.21) | copy-start | bytes 147460
  90.2 26.2 %copy-start.5 = (f32[256,256]{1,0:T(8,128)S(1)}, f32[256,256]{1,0:T(8,128)}, u32[]{:S(2)}) copy-start(f32[256,256]{1,0:T(8,128)} %param.17) | copy-start | bytes 786436
  90.5 39.3 %copy-start.1 = (bf16[3,256,256]{2,1,0:T(8,128)(2,1)S(1)}, bf16[3,256,256]{2,1,0:T(8,128)(2,1)}, u32[]{:S(2)}) copy-start(bf16[3,256,256]{2,1,0:T(8,128)(2,1)} %param.16) | copy-start | bytes 1179652
  92.1 19.6 %all-to-all-start = ((f32[16,16,768]{2,1,0:T(8,128)}), f32[16,16,768]{2,1,0:T(8,128)S(1)}, u32[]{:S(2)}, u32[]{:S(2)}) async-start(f32[16,16,768]{2,1,0:T(8,128)} %bitcast.4), calls=%async_computation | async-start | bytes 1572864 | tf_op jit(solution)/shard_map/all_to_all | solution.py:25
  112.8 17.0 %all-to-all-start.1 = ((f32[16,16,768]{2,1,0:T(8,128)}), f32[16,16,768]{2,1,0:T(8,128)S(1)}, u32[]{:S(2)}, u32[]{:S(2)}) async-start(f32[16,16,768]{2,1,0:T(8,128)} %broadcast_in_dim.6), calls=%async_computation.1 | async-start | bytes 1572864 | tf_op jit(solution)/shard_map/all_to_all | solution.py:31
  132.0 9.5 %all-to-all-start.2 = ((f32[8,1,1]{2,1,0:T(1,128)}), f32[8,1,1]{2,1,0:T(1,128)S(1)}, u32[]{:S(2)}, u32[]{:S(2)}) async-start(f32[8,1,1]{2,1,0:T(1,128)} %broadcast_in_dim.7), calls=%async_computation.2 | async-start | bytes 8192 | tf_op jit(solution)/shard_map/all_to_all | solution.py:31
  136.3 73.9 %all-gather.5.cloned.1.call-start = ((), (), s32[]{:S(2)}) async-start(), calls=%async_computation.4 | async-start | bytes 6684672 | tf_op jit(solution)/shard_map/all_gather | solution.py:53
  143.2 72.6 %copy-start.4 = (f32[256,256]{1,0:T(8,128)}, f32[256,256]{1,0:T(8,128)S(1)}, u32[]{:S(2)}) copy-start(f32[256,256]{1,0:T(8,128)S(1)} %copy.104) | copy-start | bytes 786436
Sparse Core Ops, SparseCore 0:
  10.1 63.8 all-gather.2
  147.4 62.7 all-gather.4
where the time goes:
time: 230 us; the launch traced here: 229 us
  waiting for transfers between devices  161 us (70%)
  matrix products  19.6 us (9%)
  local copies, waits for them, and re-layouts  16.7 us (7%)
  between operations  15.1 us (7%)
  starting transfers between devices  13.2 us (6%)
  other arithmetic  3.98 us (2%)
    all_gather x1, waiting for transfers between devices, shards(): pieces = lax.all_gather(factors, 'fs', axis=1, tiled=True)  66.2 us
    all_gather x1, waiting for transfers between devices, rows_first(): lax.all_gather(both, axis, axis=0, tiled=True)  61.5 us
    all_to_all x2, waiting for transfers between devices, from_everyone(): return lax.all_to_all(copies, axis, split_axis=0, concat_axis=0, tiled=True)  18 us
    all_to_all x1, waiting for transfers between devices, sum_at_owner(): lax.all_to_all(pieces, axis, split_axis=0, concat_axis=0, tiled=True)  14.2 us
    all_to_all x2, starting transfers between devices, from_everyone(): return lax.all_to_all(copies, axis, split_axis=0, concat_axis=0, tiled=True)  7.9 us
    unnamed x27, local copies, waits for them, and re-layouts  7.66 us
    dot_general x1, matrix products, shards(): jnp.dot(inputs, pieces[0], preferred_element_type=jnp.float32)  6.46 us
    transpose x1, local copies, waits for them, and re-layouts, rows_first(): gathered.append(jnp.moveaxis(share, 0, dim))  5.54 us
  transfers between devices with their start and end apart: 5, of which 5 were waited for; matrix products, arithmetic and copies ran while one was open for 1% of the time, Pallas kernels for 0%

commit v1 on v0

v1 whole, which is shorter than its diff:
```python
import functools

import jax
import jax.numpy as jnp
from jax import lax
from jax.experimental import pallas as pl
from jax.experimental.pallas import tpu as pltpu
from jax.sharding import PartitionSpec as P

C = 2048
RANK = 256
FIRST_DECAY = 0.9
SECOND_DECAY = 0.95
DIVISOR_EPS = 1e-08
SQUARE_EPS = 1e-06
LEARN_RATE = 0.01

SIDE = 4
FS = SIDE * SIDE
TP = 8
W = 256
RS = RANK // FS
TOK = 1024
D = 4096
MESH = pl.DeviceIdType.MESH
F32 = jnp.float32
BF16 = jnp.bfloat16

MESSAGES = []
for _k in (0, 1):
    for _d in (1, -1):
        MESSAGES.append((_k, 1, 0, _d))
        MESSAGES.append((_k, 2, 0, _d))
        for _po in (0, -1, 1, 2):
            MESSAGES.append((_k, 3, _po, _d))
            MESSAGES.append((_k, 4, _po, _d))
INDEX = {message: at for at, message in enumerate(MESSAGES)}
COUNT = len(MESSAGES)


class RingGather:
    def __init__(self, me, part, send, recv):
        self.z, self.x = me // SIDE, lax.rem(me, SIDE)
        self.part, self.send, self.recv = part, send, recv

    def slot(self, k, po, qo):
        dx, dz = (po, qo) if k == 0 else (qo, po)
        z = lax.rem(self.z + dz + SIDE, SIDE)
        x = lax.rem(self.x + dx + SIDE, SIDE)
        return z * SIDE + x

    def copy(self, message, received):
        k, stage, po, d = message
        if stage == 1:
            at, half, first = (0, 0), None, True
        elif stage == 2:
            at, half, first = (-d, 0), 0 if d > 0 else 1, True
        elif stage == 3:
            at, half, first = (po, 0), None, False
        else:
            at, half, first = (po, -d), 0 if d > 0 else 1, False
        to = self.slot(k, d, 0) if first else self.slot(k, 0, d)
        if received:
            at = (at[0] - d, at[1]) if first else (at[0], at[1] - d)
        at = tuple((o + 1) % SIDE - 1 for o in at)
        ref = self.part(self.slot(k, *at), k, half)
        index = INDEX[message]
        return pltpu.make_async_remote_copy(
            src_ref=ref,
            dst_ref=ref,
            send_sem=self.send.at[index],
            recv_sem=self.recv.at[index],
            device_id={"fs": to},
            device_id_type=MESH,
        )

    def start(self, *message):
        self.copy(message, False).start()

    def wait(self, *message):
        self.copy(message, True).wait_recv()

    def run(self, arrived):
        for stage in (1, 3):
            for d in (1, -1):
                for k in (0, 1):
                    self.start(k, stage, 0, d)
        for d in (1, -1):
            for k in (0, 1):
                self.wait(k, 1, 0, d)
                self.start(k, 2, 0, d)
                self.start(k, 3, -d, 1)
                self.start(k, 3, -d, -1)
                arrived(k, -d, 0)
        for d in (1, -1):
            for k in (0, 1):
                self.wait(k, 3, 0, d)
                self.start(k, 4, 0, d)
                arrived(k, 0, -d)
        for k in (0, 1):
            self.wait(k, 2, 0, 1)
            self.wait(k, 2, 0, -1)
            self.start(k, 3, 2, 1)
            self.start(k, 3, 2, -1)
            arrived(k, 2, 0)
        for po in (-1, 1):
            for d in (1, -1):
                for k in (0, 1):
                    self.wait(k, 3, po, d)
                    self.start(k, 4, po, d)
                    arrived(k, po, -d)
        for k in (0, 1):
            self.wait(k, 4, 0, 1)
            self.wait(k, 4, 0, -1)
            arrived(k, 0, 2)
        for d in (1, -1):
            for k in (0, 1):
                self.wait(k, 3, 2, d)
                self.start(k, 4, 2, d)
                arrived(k, 2, -d)
        for po in (-1, 1, 2):
            for k in (0, 1):
                self.wait(k, 4, po, 1)
                self.wait(k, 4, po, -1)
                arrived(k, po, 2)

    def finish(self):
        for message in MESSAGES:
            self.copy(message, False).wait_send()


def high_low(values):
    upper = values.astype(BF16)
    return upper, (values - upper.astype(F32)).astype(BF16)


def kernel(
    inputs,
    value_cot,
    gate_cot,
    out_cot,
    conv_output,
    factors,
    value_weight,
    gate_weight,
    out_weight,
    first_moment,
    second_moment,
    first_out,
    second_out,
    value_update,
    gate_update,
    out_update,
    value_copy,
    gate_copy,
    out_copy,
    inp,
    oct_,
    cots,
    cots_t,
    fbuf,
    wbuf,
    mom,
    summed,
    pieces,
    arrived_pieces,
    dirs,
    sums,
    upd,
    copies,
    local_sem,
    out_sem,
    f_send,
    f_recv,
    core_send,
    core_recv,
    a_send,
    a_recv,
    d_send,
    d_recv,
    s_send,
    s_recv,
    c_send,
    c_recv,
):
    me = lax.axis_index("fs")
    t = lax.axis_index("tp")
    core = lax.rem(t, 2)
    partner = t + 1 - 2 * core

    loads = []

    def load(src, dst):
        copy = pltpu.make_async_copy(src, dst, local_sem.at[len(loads)])
        copy.start()
        loads.append(copy)

    load(factors, fbuf.at[me])
    load(inputs, inp)
    load(out_cot, oct_)
    load(value_cot, cots.at[0])
    load(gate_cot, cots.at[1])
    load(conv_output, cots.at[2])
    load(first_moment, mom.at[0])
    load(second_moment, mom.at[1])
    load(value_weight, wbuf.at[0])
    load(gate_weight, wbuf.at[1])
    load(out_weight, wbuf.at[2])

    barrier = pltpu.get_barrier_semaphore()

    def greet_fs(j, _):
        pl.semaphore_signal(
            barrier, inc=1, device_id={"fs": lax.rem(me + j, FS)}, device_id_type=MESH
        )
        return _

    def greet_tp(j, _):
        pl.semaphore_signal(
            barrier, inc=1, device_id={"tp": lax.rem(t + j, TP)}, device_id_type=MESH
        )
        return _

    lax.fori_loop(1, FS, greet_fs, 0)
    lax.fori_loop(1, TP, greet_tp, 0)
    pl.semaphore_wait(barrier, FS - 1 + TP - 1)

    def factor_part(of_core):
        def part(s, k, half):
            at = of_core * 128 + 64 * k
            size = 64
            if half is not None:
                at, size = at + 32 * half, 32
            return fbuf.at[s, :, pl.ds(pl.multiple_of(at, 32), size), :]

        return part

    ring = RingGather(me, factor_part(core), f_send, f_recv)

    def share(k, po, qo, mine):
        at = (po + 1) * SIDE + (qo + 1) + FS * k
        ref = factor_part(core if mine else 1 - core)(ring.slot(k, po, qo), k, None)
        return pltpu.make_async_remote_copy(
            src_ref=ref,
            dst_ref=ref,
            send_sem=core_send.at[at],
            recv_sem=core_recv.at[at],
            device_id={"tp": partner},
            device_id_type=MESH,
        )

    def multiply(s, first):
        cols = pl.ds(pl.multiple_of(s * W, W), W)

        def tile(i, _):
            rows = pl.ds(pl.multiple_of(i * 256, 256), 256)
            left = inp[rows, cols]
            other = oct_[rows, cols]
            for m in range(3):
                product = jnp.dot(
                    other if m == 2 else left, fbuf[s, m], preferred_element_type=F32
                )
                if first:
                    summed[m, rows, :] = product
                else:
                    summed[m, rows, :] += product
            return _

        lax.fori_loop(0, TOK // 256, tile, 0)

    parts_here = {}

    def turn_cots():
        for copy in loads[3:6]:
            copy.wait()
        for m in range(3):

            def turn(i, _):
                rows = pl.ds(pl.multiple_of(i * 256, 256), 256)
                cots_t[m, :, rows] = cots[m, rows, :].T
                return _

            lax.fori_loop(0, TOK // 256, turn, 0)

    def factor_arrived(k, po, qo):
        share(k, po, qo, True).start()
        dx, dz = (po, qo) if k == 0 else (qo, po)
        if (dx, dz) not in parts_here:
            parts_here[dx, dz] = 1
            return
        for kk in (0, 1):
            pq = (dx, dz) if kk == 0 else (dz, dx)
            share(kk, *pq, False).wait_recv()
        multiply(ring.slot(0, dx, dz), False)

    loads[0].wait()

    class First:
        done = False

    def on_factor(k, po, qo):
        if not First.done:
            First.done = True
            turn_cots()
            loads[1].wait()
            loads[2].wait()
            multiply(me, True)
        factor_arrived(k, po, qo)

    ring.run(on_factor)

    for m in range(3):
        upper, lower = high_low(summed[m])
        product = jnp.dot(cots_t[m], upper, preferred_element_type=F32)
        product += jnp.dot(cots_t[m], lower, preferred_element_type=F32)
        pieces[:, m, :, :] = product.T.reshape(FS, RS, W)

    def to_owner(j):
        peer = lax.rem(me + j, FS)
        return pltpu.make_async_remote_copy(
            src_ref=pieces.at[peer],
            dst_ref=arrived_pieces.at[me],
            send_sem=a_send.at[j],
            recv_sem=a_recv.at[j],
            device_id={"fs": peer},
            device_id_type=MESH,
        )

    def from_peer(j):
        source = lax.rem(me - j + FS, FS)
        return pltpu.make_async_remote_copy(
            src_ref=pieces.at[source],
            dst_ref=arrived_pieces.at[source],
            send_sem=a_send.at[j],
            recv_sem=a_recv.at[j],
            device_id={"fs": source},
            device_id_type=MESH,
        )

    def loop(start, stop, step):
        def body(j, carry):
            step(j)
            return carry

        lax.fori_loop(start, stop, body, 0)

    loop(1, FS, lambda j: to_owner(j).start())

    def add_piece(j, total):
        from_peer(j).wait_recv()
        return total + arrived_pieces[lax.rem(me - j + FS, FS)]

    projected = lax.fori_loop(1, FS, add_piece, pieces[me])

    loads[6].wait()
    loads[7].wait()
    new_first = FIRST_DECAY * mom[0] + (1.0 - FIRST_DECAY) * projected
    new_second = SECOND_DECAY * mom[1] + (1.0 - SECOND_DECAY) * projected * projected
    dirs[me] = new_first / (jnp.sqrt(new_second) + DIVISOR_EPS)
    mom[0] = new_first
    mom[1] = new_second

    def direction(j, received):
        source = lax.rem(me - j + FS, FS) if received else me
        return pltpu.make_async_remote_copy(
            src_ref=dirs.at[source],
            dst_ref=dirs.at[source],
            send_sem=d_send.at[j],
            recv_sem=d_recv.at[j],
            device_id={"fs": lax.rem(me + j, FS)},
            device_id_type=MESH,
        )

    loop(1, FS, lambda j: direction(j, False).start())

    stores = []

    def store(src, dst):
        copy = pltpu.make_async_copy(src, dst, out_sem.at[len(stores)])
        copy.start()
        stores.append(copy)

    store(mom.at[0], first_out)
    store(mom.at[1], second_out)

    loop(1, FS, lambda j: direction(j, True).wait_recv())

    def square(s, total):
        block = dirs[s].reshape(3 * RS // 8, 8, W)
        return total + jnp.sum(block * block, axis=0)

    squares = lax.fori_loop(0, FS, square, jnp.zeros((8, W), F32))
    sums[t] = squares[:, :128] + squares[:, 128:]

    def scalar(j, received):
        source = lax.rem(t - j + TP, TP) if received else t
        return pltpu.make_async_remote_copy(
            src_ref=sums.at[source],
            dst_ref=sums.at[source],
            send_sem=s_send.at[j],
            recv_sem=s_recv.at[j],
            device_id={"tp": lax.rem(t + j, TP)},
            device_id_type=MESH,
        )

    loop(1, TP, lambda j: scalar(j, False).start())

    unscaled = []
    for m in range(3):
        whole = dirs[:, m, :, :].reshape(RANK, W)
        if m == 2:
            upper, lower = high_low(whole.T)
            contract = (((1,), (1,)), ((), ()))
            own = fbuf[me, m]
            update = lax.dot_general(upper, own, contract, preferred_element_type=F32)
            update += lax.dot_general(lower, own, contract, preferred_element_type=F32)
        else:
            upper, lower = high_low(whole)
            update = jnp.dot(fbuf[me, m], upper, preferred_element_type=F32)
            update += jnp.dot(fbuf[me, m], lower, preferred_element_type=F32)
        upd[m] = update
    for copy in loads[8:]:
        copy.wait()
    loop(1, TP, lambda j: scalar(j, True).wait_recv())
    total = jnp.sum(jnp.sum(sums[...], axis=0), keepdims=True)
    norm_scale = lax.rsqrt(total / (3 * RANK * C) + SQUARE_EPS)
    for m in range(3):
        update = norm_scale * upd[m]
        upd[m] = update
        copies[me, m] = (wbuf[m] - LEARN_RATE * update).astype(BF16)

    def copy_part(s, k, half):
        at, size = 128 * k, 128
        if half is not None:
            at, size = at + 64 * half, 64
        return copies.at[s, :, pl.ds(at, size), :]

    gather = RingGather(me, copy_part, c_send, c_recv)

    def store_block(s):
        at = pl.ds(pl.multiple_of(s * W, W), W)
        store(copies.at[s, 0], value_copy.at[at, :])
        store(copies.at[s, 1], gate_copy.at[at, :])
        store(copies.at[s, 2], out_copy.at[:, at])

    blocks = {}

    def copy_arrived(k, po, qo):
        dx, dz = (po, qo) if k == 0 else (qo, po)
        if not blocks:
            for m, ref in enumerate((value_update, gate_update, out_update)):
                store(upd.at[m], ref)
            store_block(me)
        if (dx, dz) in blocks:
            store_block(gather.slot(0, dx, dz))
        blocks[dx, dz] = 1

    gather.run(copy_arrived)

    gather.finish()
    ring.finish()
    for k in (0, 1):
        for po in (-1, 0, 1, 2):
            for qo in (-1, 0, 1, 2):
                if (po, qo) != (0, 0):
                    share(k, po, qo, True).wait_send()
    loop(1, FS, lambda j: to_owner(j).wait_send())
    loop(1, FS, lambda j: direction(j, False).wait_send())
    loop(1, TP, lambda j: scalar(j, False).wait_send())
    for copy in stores:
        copy.wait()


def shards(*args):
    anywhere = pl.BlockSpec(memory_space=pl.ANY)
    dma = pltpu.SemaphoreType.DMA
    return pl.pallas_call(
        kernel,
        out_shape=(
            jax.ShapeDtypeStruct((3, RS, W), F32),
            jax.ShapeDtypeStruct((3, RS, W), F32),
            jax.ShapeDtypeStruct((W, W), F32),
            jax.ShapeDtypeStruct((W, W), F32),
            jax.ShapeDtypeStruct((W, W), F32),
            jax.ShapeDtypeStruct((D, W), BF16),
            jax.ShapeDtypeStruct((D, W), BF16),
            jax.ShapeDtypeStruct((W, D), BF16),
        ),
        in_specs=[anywhere] * 11,
        out_specs=(anywhere,) * 8,
        scratch_shapes=[
            pltpu.VMEM((TOK, D), BF16),
            pltpu.VMEM((TOK, D), BF16),
            pltpu.VMEM((3, TOK, W), BF16),
            pltpu.VMEM((3, W, TOK), BF16),
            pltpu.VMEM((FS, 3, W, RANK), BF16),
            pltpu.VMEM((3, W, W), F32),
            pltpu.VMEM((2, 3, RS, W), F32),
            pltpu.VMEM((3, TOK, RANK), F32),
            pltpu.VMEM((FS, 3, RS, W), F32),
            pltpu.VMEM((FS, 3, RS, W), F32),
            pltpu.VMEM((FS, 3, RS, W), F32),
            pltpu.VMEM((TP, 8, 128), F32),
            pltpu.VMEM((3, W, W), F32),
            pltpu.VMEM((FS, 3, W, W), BF16),
            dma((11,)),
            dma((5 + 3 * FS,)),
            dma((COUNT,)),
            dma((COUNT,)),
            dma((2 * FS,)),
            dma((2 * FS,)),
            dma((FS,)),
            dma((FS,)),
            dma((FS,)),
            dma((FS,)),
            dma((TP,)),
            dma((TP,)),
            dma((COUNT,)),
            dma((COUNT,)),
        ],
        compiler_params=pltpu.CompilerParams(
            collective_id=0, has_side_effects=True, vmem_limit_bytes=60 * 1024 * 1024
        ),
    )(*args)


def solution(mesh):
    placed = (
        P("fs", None),
        P("fs", "tp"),
        P("fs", "tp"),
        P("fs", None),
        P("fs", "tp"),
        P(None, "fs", None),
        P("fs", "tp"),
        P("fs", "tp"),
        P("tp", "fs"),
        P(None, "fs", "tp"),
        P(None, "fs", "tp"),
    )
    return jax.shard_map(
        shards,
        mesh=mesh,
        in_specs=placed,
        out_specs=(
            P(None, "fs", "tp"),
            P(None, "fs", "tp"),
            P("fs", "tp"),
            P("fs", "tp"),
            P("tp", "fs"),
            P(None, "tp"),
            P(None, "tp"),
            P("tp", None),
        ),
        check_vma=False,
    )
```

time: 230 us -> 133 us (0.58)
  waiting for transfers between devices: 161 us -> 0 us
  Pallas kernels: 0 us -> 117 us
  matrix products: 19.6 us -> 0 us
  between operations: 15.1 us -> 0.65 us
  starting transfers between devices: 13.2 us -> 0 us
  other arithmetic: 3.98 us -> 0 us
    all_gather x2 -> x0, waiting for transfers between devices: 128 us -> none  [the longest x1 66.2 us: shards(): pieces = lax.all_gather(factors, 'fs', axis=1, tiled=True)]
    pallas_call x0 -> x1, Pallas kernels: none -> 117 us  [shards(): pl.pallas_call(kernel, out_shape=(jax.ShapeDtypeStruct((3, RS, W), F32),...]
    all_to_all x3 -> x0, waiting for transfers between devices: 32.2 us -> none  [the longest x2 18 us: from_everyone(): return lax.all_to_all(copies, axis, split_axis=0, concat_axis=0, tiled=True)]
    dot_general x15 -> x0, matrix products: 19.6 us -> none  [the longest x1 6.46 us: shards(): jnp.dot(inputs, pieces[0], preferred_element_type=jnp.float32)]
    all_to_all x3 -> x0, starting transfers between devices: 13.2 us -> none  [the longest x2 7.9 us: from_everyone(): return lax.all_to_all(copies, axis, split_axis=0, concat_axis=0, tiled=True)]
    unnamed x27 -> x12, local copies, waits for them, and re-layouts: 7.66 us -> 14.7 us
    transpose x1 -> x0, local copies, waits for them, and re-layouts: 5.54 us -> none  [rows_first(): gathered.append(jnp.moveaxis(share, 0, dim))]
  transfers between devices with their start and end apart: 5 -> 0, of which waited for: 5 -> 0; matrix products, arithmetic and copies ran while one was open for 1% -> 0% of each run, Pallas kernels for 0% -> 0%
where the time goes in v1:
time: 133 us; the launch traced here: 132 us
  Pallas kernels  117 us (88%)
  local copies, waits for them, and re-layouts  14.7 us (11%)
    pallas_call x1, Pallas kernels, shards(): pl.pallas_call(kernel, out_shape=(jax.ShapeDtypeStruct((3, RS, W), F32),...  117 us
    unnamed x12, local copies, waits for them, and re-layouts  14.7 us

profile of v1, /device:TPU:0, one launch (start us, length us, event | category | flops | bytes accessed | tf_op | source)
XLA Modules:
  0.0 132.4 jit_solution(11820322226941772125)
XLA Ops:
  0.6 117.0 %shard_map.170 = (f32[3,16,256]{2,1,0:T(8,128)}, f32[3,16,256]{2,1,0:T(8,128)}, f32[256,256]{1,0:T(8,128)}, f32[256,256]{1,0:T(8,128)}, f32[256,256]{1,0:T(8,128...) custom-call(bf16[1024,4096]{1,0:T(8,128)(2,1)} %inputs.1, ...), custom_call_target="tpu_custom_call" | custom-call | tf_op jit(solution)/shard_map/pallas_call | solution.py:477
  117.6 1.4 %copy.27 = f32[3,16,256]{2,1,0:T(8,128)} copy(f32[3,16,256]{2,1,0:T(8,128)} %get-tuple-element.16) | data formatting | bytes 98304
  119.1 1.4 %copy.28 = f32[3,16,256]{2,1,0:T(8,128)} copy(f32[3,16,256]{2,1,0:T(8,128)} %get-tuple-element.17) | data formatting | bytes 98304
  120.5 1.7 %copy.29 = f32[256,256]{1,0:T(8,128)} copy(f32[256,256]{1,0:T(8,128)} %get-tuple-element.18) | data formatting | bytes 524288
  122.2 1.7 %copy.30 = f32[256,256]{1,0:T(8,128)} copy(f32[256,256]{1,0:T(8,128)} %get-tuple-element.19) | data formatting | bytes 524288
  123.8 1.7 %copy.31 = f32[256,256]{1,0:T(8,128)} copy(f32[256,256]{1,0:T(8,128)} %get-tuple-element.20) | data formatting | bytes 524288
  125.5 0.0 copy-start.1
  125.5 3.2 %copy.32 = bf16[4096,256]{1,0:T(8,128)(2,1)} copy(bf16[4096,256]{1,0:T(8,128)(2,1)} %get-tuple-element.21) | data formatting | bytes 4194304
  128.7 0.0 copy-done.1
  128.7 0.0 copy-start
  128.7 1.3 copy.33
  130.0 1.0 copy-done
  131.0 1.3 copy.34
Async XLA Ops:
  125.5 3.2 %copy-start.1 = (bf16[4096,256]{1,0:T(8,128)(2,1)S(1)}, bf16[4096,256]{1,0:T(8,128)(2,1)}, u32[]{:S(2)}) copy-start(bf16[4096,256]{1,0:T(8,128)(2,1)} %get-tuple-element.22) | copy-start | bytes 6291460
  128.7 2.3 %copy-start = (bf16[256,4096]{1,0:T(8,128)(2,1)S(1)}, bf16[256,4096]{1,0:T(8,128)(2,1)}, u32[]{:S(2)}) copy-start(bf16[256,4096]{1,0:T(8,128)(2,1)} %get-tuple-element.23) | copy-start | bytes 6291460

commit v2 on v1

--- a/solution.py
+++ b/solution.py
@@ -78,7 +78,8 @@
         self.copy(message, False).start()
 
     def wait(self, *message):
-        self.copy(message, True).wait_recv()
+        with jax.named_scope("wait_{}_{}_{}_{}".format(*message)):
+            self.copy(message, True).wait_recv()
 
     def run(self, arrived):
         for stage in (1, 3):
@@ -146,30 +147,22 @@
     out_weight,
     first_moment,
     second_moment,
-    first_out,
-    second_out,
-    value_update,
-    gate_update,
-    out_update,
-    value_copy,
-    gate_copy,
-    out_copy,
+    mom,
+    upd,
+    copies,
     inp,
     oct_,
     cots,
     cots_t,
     fbuf,
     wbuf,
-    mom,
     summed,
     pieces,
     arrived_pieces,
     dirs,
     sums,
-    upd,
-    copies,
+    fs_sums,
     local_sem,
-    out_sem,
     f_send,
     f_recv,
     core_send,
@@ -180,6 +173,8 @@
     d_recv,
     s_send,
     s_recv,
+    q_send,
+    q_recv,
     c_send,
     c_recv,
 ):
@@ -196,11 +191,11 @@
         loads.append(copy)
 
     load(factors, fbuf.at[me])
-    load(inputs, inp)
-    load(out_cot, oct_)
     load(value_cot, cots.at[0])
     load(gate_cot, cots.at[1])
     load(conv_output, cots.at[2])
+    load(inputs, inp)
+    load(out_cot, oct_)
     load(first_moment, mom.at[0])
     load(second_moment, mom.at[1])
     load(value_weight, wbuf.at[0])
@@ -223,7 +218,21 @@
 
     lax.fori_loop(1, FS, greet_fs, 0)
     lax.fori_loop(1, TP, greet_tp, 0)
-    pl.semaphore_wait(barrier, FS - 1 + TP - 1)
+
+    with jax.named_scope("turn"):
+        for copy in loads[1:4]:
+            copy.wait()
+        for m in range(3):
+
+            def turn(i, _):
+                rows = pl.ds(pl.multiple_of(i * 256, 256), 256)
+                cots_t[m, :, rows] = cots[m, rows, :].T
+                return _
+
+            lax.fori_loop(0, TOK // 256, turn, 0)
+
+    with jax.named_scope("barrier"):
+        pl.semaphore_wait(barrier, FS - 1 + TP - 1)
 
     def factor_part(of_core):
         def part(s, k, half):
@@ -253,7 +262,7 @@
         cols = pl.ds(pl.multiple_of(s * W, W), W)
 
         def tile(i, _):
-            rows = pl.ds(pl.multiple_of(i * 256, 256), 256)
+            rows = pl.ds(pl.multiple_of(i * 512, 512), 512)
             left = inp[rows, cols]
             other = oct_[rows, cols]
             for m in range(3):
@@ -266,54 +275,50 @@
                     summed[m, rows, :] += product
             return _
 
-        lax.fori_loop(0, TOK // 256, tile, 0)
-
-    parts_here = {}
-
-    def turn_cots():
-        for copy in loads[3:6]:
-            copy.wait()
-        for m in range(3):
-
-            def turn(i, _):
-                rows = pl.ds(pl.multiple_of(i * 256, 256), 256)
-                cots_t[m, :, rows] = cots[m, rows, :].T
-                return _
-
-            lax.fori_loop(0, TOK // 256, turn, 0)
-
-    def factor_arrived(k, po, qo):
+        with jax.named_scope("multiply"):
+            lax.fori_loop(0, TOK // 512, tile, 0)
+
+    loads[0].wait()
+    halves = set()
+    waiting = []
+
+    def multiply_next():
+        if not waiting:
+            return
+        offsets = waiting.pop(0)
+        if offsets is None:
+            with jax.named_scope("wait_loads"):
+                loads[4].wait()
+                loads[5].wait()
+            multiply(me, True)
+            return
+        dx, dz = offsets
+        with jax.named_scope("wait_share"):
+            share(0, dx, dz, False).wait_recv()
+            share(1, dz, dx, False).wait_recv()
+        multiply(ring.slot(0, dx, dz), False)
+
+    waiting.append(None)
+
+    def on_factor(k, po, qo):
         share(k, po, qo, True).start()
-        dx, dz = (po, qo) if k == 0 else (qo, po)
-        if (dx, dz) not in parts_here:
-            parts_here[dx, dz] = 1
+        offsets = (po, qo) if k == 0 else (qo, po)
+        if offsets not in halves:
+            halves.add(offsets)
             return
-        for kk in (0, 1):
-            pq = (dx, dz) if kk == 0 else (dz, dx)
-            share(kk, *pq, False).wait_recv()
-        multiply(ring.slot(0, dx, dz), False)
-
-    loads[0].wait()
-
-    class First:
-        done = False
-
-    def on_factor(k, po, qo):
-        if not First.done:
-            First.done = True
-            turn_cots()
-            loads[1].wait()
-            loads[2].wait()
-            multiply(me, True)
-        factor_arrived(k, po, qo)
+        multiply_next()
+        waiting.append(offsets)
 
     ring.run(on_factor)
+    while waiting:
+        multiply_next()
 
     for m in range(3):
-        upper, lower = high_low(summed[m])
-        product = jnp.dot(cots_t[m], upper, preferred_element_type=F32)
-        product += jnp.dot(cots_t[m], lower, preferred_element_type=F32)
-        pieces[:, m, :, :] = product.T.reshape(FS, RS, W)
+        with jax.named_scope("project"):
+            upper, lower = high_low(summed[m])
+            product = jnp.dot(cots_t[m], upper, preferred_element_type=F32)
+            product += jnp.dot(cots_t[m], lower, preferred_element_type=F32)
+            pieces[:, m, :, :] = product.T.reshape(FS, RS, W)
 
     def to_owner(j):
         peer = lax.rem(me + j, FS)
@@ -350,7 +355,8 @@
         from_peer(j).wait_recv()
         return total + arrived_pieces[lax.rem(me - j + FS, FS)]
 
-    projected = lax.fori_loop(1, FS, add_piece, pieces[me])
+    with jax.named_scope("sum_pieces"):
+        projected = lax.fori_loop(1, FS, add_piece, pieces[me])
 
     loads[6].wait()
     loads[7].wait()
@@ -373,23 +379,8 @@
 
     loop(1, FS, lambda j: direction(j, False).start())
 
-    stores = []
-
-    def store(src, dst):
-        copy = pltpu.make_async_copy(src, dst, out_sem.at[len(stores)])
-        copy.start()
-        stores.append(copy)
-
-    store(mom.at[0], first_out)
-    store(mom.at[1], second_out)
-
-    loop(1, FS, lambda j: direction(j, True).wait_recv())
-
-    def square(s, total):
-        block = dirs[s].reshape(3 * RS // 8, 8, W)
-        return total + jnp.sum(block * block, axis=0)
-
-    squares = lax.fori_loop(0, FS, square, jnp.zeros((8, W), F32))
+    own = dirs[me].reshape(3 * RS // 8, 8, W)
+    squares = jnp.sum(own * own, axis=0)
     sums[t] = squares[:, :128] + squares[:, 128:]
 
     def scalar(j, received):
@@ -403,9 +394,25 @@
             device_id_type=MESH,
         )
 
+    def fs_scalar(j, received):
+        source = lax.rem(me - j + FS, FS) if received else me
+        return pltpu.make_async_remote_copy(
+            src_ref=fs_sums.at[source],
+            dst_ref=fs_sums.at[source],
+            send_sem=q_send.at[j],
+            recv_sem=q_recv.at[j],
+            device_id={"fs": lax.rem(me + j, FS)},
+            device_id_type=MESH,
+        )
+
     loop(1, TP, lambda j: scalar(j, False).start())
-
-    unscaled = []
+    with jax.named_scope("wait_scalar"):
+        loop(1, TP, lambda j: scalar(j, True).wait_recv())
+    fs_sums[me] = jnp.sum(sums[...], axis=0)
+    loop(1, FS, lambda j: fs_scalar(j, False).start())
+    with jax.named_scope("wait_directions"):
+        loop(1, FS, lambda j: direction(j, True).wait_recv())
+
     for m in range(3):
         whole = dirs[:, m, :, :].reshape(RANK, W)
         if m == 2:
@@ -421,8 +428,9 @@
         upd[m] = update
     for copy in loads[8:]:
         copy.wait()
-    loop(1, TP, lambda j: scalar(j, True).wait_recv())
-    total = jnp.sum(jnp.sum(sums[...], axis=0), keepdims=True)
+    with jax.named_scope("wait_fs_scalar"):
+        loop(1, FS, lambda j: fs_scalar(j, True).wait_recv())
+    total = jnp.sum(jnp.sum(fs_sums[...], axis=0), keepdims=True)
     norm_scale = lax.rsqrt(total / (3 * RANK * C) + SQUARE_EPS)
     for m in range(3):
         update = norm_scale * upd[m]
@@ -437,45 +445,125 @@
 
     gather = RingGather(me, copy_part, c_send, c_recv)
 
-    def store_block(s):
+    gather.run(lambda k, po, qo: None)
+
+    with jax.named_scope("finish"):
+        gather.finish()
+    with jax.named_scope("finish_rest"):
+        ring.finish()
+        for k in (0, 1):
+            for po in (-1, 0, 1, 2):
+                for qo in (-1, 0, 1, 2):
+                    if (po, qo) != (0, 0):
+                        share(k, po, qo, True).wait_send()
+        loop(1, FS, lambda j: to_owner(j).wait_send())
+        loop(1, FS, lambda j: direction(j, False).wait_send())
+        loop(1, TP, lambda j: scalar(j, False).wait_send())
+        loop(1, FS, lambda j: fs_scalar(j, False).wait_send())
+
+
+def store_kernel(
+    mom,
+    upd,
+    copies,
+    first_out,
+    second_out,
+    value_update,
+    gate_update,
+    out_update,
+    value_copy,
+    gate_copy,
+    out_copy,
+    sem,
+    block_sem,
+):
+    small = [
+        pltpu.make_async_copy(src, dst, sem.at[i])
+        for i, (src, dst) in enumerate(
+            (
+                (mom.at[0], first_out),
+                (mom.at[1], second_out),
+                (upd.at[0], value_update),
+                (upd.at[1], gate_update),
+                (upd.at[2], out_update),
+            )
+        )
+    ]
+
+    def block(s):
         at = pl.ds(pl.multiple_of(s * W, W), W)
-        store(copies.at[s, 0], value_copy.at[at, :])
-        store(copies.at[s, 1], gate_copy.at[at, :])
-        store(copies.at[s, 2], out_copy.at[:, at])
-
-    blocks = {}
-
-    def copy_arrived(k, po, qo):
-        dx, dz = (po, qo) if k == 0 else (qo, po)
-        if not blocks:
-            for m, ref in enumerate((value_update, gate_update, out_update)):
-                store(upd.at[m], ref)
-            store_block(me)
-        if (dx, dz) in blocks:
-            store_block(gather.slot(0, dx, dz))
-        blocks[dx, dz] = 1
-
-    gather.run(copy_arrived)
-
-    gather.finish()
-    ring.finish()
-    for k in (0, 1):
-        for po in (-1, 0, 1, 2):
-            for qo in (-1, 0, 1, 2):
-                if (po, qo) != (0, 0):
-                    share(k, po, qo, True).wait_send()
-    loop(1, FS, lambda j: to_owner(j).wait_send())
-    loop(1, FS, lambda j: direction(j, False).wait_send())
-    loop(1, TP, lambda j: scalar(j, False).wait_send())
-    for copy in stores:
+        return [
+            pltpu.make_async_copy(copies.at[s, 0], value_copy.at[at, :], block_sem.at[s, 0]),
+            pltpu.make_async_copy(copies.at[s, 1], gate_copy.at[at, :], block_sem.at[s, 1]),
+            pltpu.make_async_copy(copies.at[s, 2], out_copy.at[:, at], block_sem.at[s, 2]),
+        ]
+
+    def start(s, carry):
+        for copy in block(s):
+            copy.start()
+        return carry
+
+    def wait(s, carry):
+        for copy in block(s):
+            copy.wait()
+        return carry
+
+    for copy in small:
+        copy.start()
+    lax.fori_loop(0, FS, start, 0)
+    lax.fori_loop(0, FS, wait, 0)
+    for copy in small:
         copy.wait()
 
 
 def shards(*args):
     anywhere = pl.BlockSpec(memory_space=pl.ANY)
+    vmem = pl.BlockSpec(memory_space=pltpu.VMEM)
     dma = pltpu.SemaphoreType.DMA
+    results = pl.pallas_call(
+        kernel,
+        out_shape=(
+            pltpu.VMEM((2, 3, RS, W), F32),
+            pltpu.VMEM((3, W, W), F32),
+            pltpu.VMEM((FS, 3, W, W), BF16),
+        ),
+        in_specs=[anywhere] * 11,
+        out_specs=(vmem,) * 3,
+        scratch_shapes=[
+            pltpu.VMEM((TOK, D), BF16),
+            pltpu.VMEM((TOK, D), BF16),
+            pltpu.VMEM((3, TOK, W), BF16),
+            pltpu.VMEM((3, W, TOK), BF16),
+            pltpu.VMEM((FS, 3, W, RANK), BF16),
+            pltpu.VMEM((3, W, W), F32),
+            pltpu.VMEM((3, TOK, RANK), F32),
+            pltpu.VMEM((FS, 3, RS, W), F32),
+            pltpu.VMEM((FS, 3, RS, W), F32),
+            pltpu.VMEM((FS, 3, RS, W), F32),
+            pltpu.VMEM((TP, 8, 128), F32),
+            pltpu.VMEM((FS, 8, 128), F32),
+            dma((11,)),
+            dma((COUNT,)),
+            dma((COUNT,)),
+            dma((2 * FS,)),
+            dma((2 * FS,)),
+            dma((FS,)),
+            dma((FS,)),
+            dma((FS,)),
+            dma((FS,)),
+            dma((TP,)),
+            dma((TP,)),
+            dma((FS,)),
+            dma((FS,)),
+            dma((COUNT,)),
+            dma((COUNT,)),
+        ],
+        compiler_params=pltpu.CompilerParams(
+            collective_id=0, has_side_effects=True, vmem_limit_bytes=48 * 1024 * 1024
+        ),
+    )(*[pltpu.with_memory_space_constraint(a, pltpu.HBM) for a in args])
     return pl.pallas_call(
-        kernel,
+        store_kernel,
         out_shape=(
             jax.ShapeDtypeStruct((3, RS, W), F32),
             jax.ShapeDtypeStruct((3, RS, W), F32),
@@ -486,42 +574,11 @@
             jax.ShapeDtypeStruct((D, W), BF16),
             jax.ShapeDtypeStruct((W, D), BF16),
         ),
-        in_specs=[anywhere] * 11,
+        in_specs=[vmem] * 3,
         out_specs=(anywhere,) * 8,
-        scratch_shapes=[
-            pltpu.VMEM((TOK, D), BF16),
-            pltpu.VMEM((TOK, D), BF16),
-            pltpu.VMEM((3, TOK, W), BF16),
-            pltpu.VMEM((3, W, TOK), BF16),
-            pltpu.VMEM((FS, 3, W, RANK), BF16),
-            pltpu.VMEM((3, W, W), F32),
-            pltpu.VMEM((2, 3, RS, W), F32),
-            pltpu.VMEM((3, TOK, RANK), F32),
-            pltpu.VMEM((FS, 3, RS, W), F32),
-            pltpu.VMEM((FS, 3, RS, W), F32),
-            pltpu.VMEM((FS, 3, RS, W), F32),
-            pltpu.VMEM((TP, 8, 128), F32),
-            pltpu.VMEM((3, W, W), F32),
-            pltpu.VMEM((FS, 3, W, W), BF16),
-            dma((11,)),
-            dma((5 + 3 * FS,)),
-            dma((COUNT,)),
-            dma((COUNT,)),
-            dma((2 * FS,)),
-            dma((2 * FS,)),
-            dma((FS,)),
-            dma((FS,)),
-            dma((FS,)),
-            dma((FS,)),
-            dma((TP,)),
-            dma((TP,)),
-            dma((COUNT,)),
-            dma((COUNT,)),
-        ],
-        compiler_params=pltpu.CompilerParams(
-            collective_id=0, has_side_effects=True, vmem_limit_bytes=60 * 1024 * 1024
-        ),
-    )(*args)
+        scratch_shapes=[dma((5,)), dma((FS, 3))],
+        compiler_params=pltpu.CompilerParams(vmem_limit_bytes=4 * 1024 * 1024),
+    )(*[pltpu.with_memory_space_constraint(r, pltpu.VMEM) for r in results])
 
 
 def solution(mesh):

time: 133 us -> 99.1 us (0.75)
  Pallas kernels: 117 us -> 98.3 us
  local copies, waits for them, and re-layouts: 14.7 us -> 0 us
    pallas_call x1 -> x2, Pallas kernels: 117 us -> 98.3 us  [the longest x1 95 us: shards(): pl.pallas_call(kernel, out_shape=(pltpu.VMEM((2, 3, RS, W), F32), pltpu.V...]
    unnamed x12 -> x0, local copies, waits for them, and re-layouts: 14.7 us -> none
where the time goes in v2:
time: 99.1 us; the launch traced here: 99 us
  Pallas kernels  98.3 us (99%)
    pallas_call x1, Pallas kernels, shards(): pl.pallas_call(kernel, out_shape=(pltpu.VMEM((2, 3, RS, W), F32), pltpu.V...  95 us
    pallas_call x1, Pallas kernels, shards(): pl.pallas_call(store_kernel, out_shape=(jax.ShapeDtypeStruct((3, RS, W),...  3.36 us

profile of v2, /device:TPU:0, one launch (start us, length us, event | category | flops | bytes accessed | tf_op | source)
XLA Modules:
  0.0 99.0 jit_solution(712581280171505340)
XLA Ops:
  0.6 95.0 %shard_map.170 = (f32[2,3,16,256]{3,2,1,0:T(8,128)S(1)}, f32[3,256,256]{2,1,0:T(8,128)S(1)}, bf16[16,3,256,256]{3,2,1,0:T(8,128)(2,1)S(1)}) custom-call(bf16[1024,4096]{1,0:T(8,128)(2,1)} %inputs.1, bf16[1024,256]{1,0:T(8,128)(2,1)} %value_cot.1, bf16[1024,256]{1,0:T(8,128)(2,1)} %gate_cot.1, bf16[1024,4096]{1,0:T(8,128)(2,1)} %out_cot.1, ...), custom_call_target="tpu_custom_call" | custom-call | tf_op jit(solution)/shard_map/pallas_call | solution.py:523
  95.6 3.4 %shard_map.171 = (f32[3,16,256]{2,1,0:T(8,128)}, f32[3,16,256]{2,1,0:T(8,128)}, f32[256,256]{1,0:T(8,128)}, f32[256,256]{1,0:T(8,128)}, f32[256,256]{1,0:T(8,128...) custom-call(f32[2,3,16,256]{3,2,1,0:T(8,128)S(1)} %get-tuple-element.11.mom, ...), custom_call_target="tpu_custom_call" | custom-call | tf_op jit(solution)/shard_map/pallas_call | solution.py:565

commit v3 on v2

v3 whole, which is shorter than its diff:
```python
import functools

import jax
import jax.numpy as jnp
from jax import lax
from jax.experimental import pallas as pl
from jax.experimental.pallas import tpu as pltpu
from jax.sharding import PartitionSpec as P

C = 2048
RANK = 256
FIRST_DECAY = 0.9
SECOND_DECAY = 0.95
DIVISOR_EPS = 1e-08
SQUARE_EPS = 1e-06
LEARN_RATE = 0.01

SIDE = 4
FS = SIDE * SIDE
TP = 8
W = 256
RS = RANK // FS
TOK = 1024
D = 4096
MESH = pl.DeviceIdType.MESH
F32 = jnp.float32
BF16 = jnp.bfloat16

RECEIVED = []
for _k in (0, 1):
    RECEIVED += [(_k, 1, 0, 1), (_k, 1, 0, -1), (_k, 2, 0, 0)]
    for _po in (0, -1, 1, 2):
        RECEIVED += [(_k, 3, _po, 1), (_k, 3, _po, -1), (_k, 4, _po, 0)]
INDEX = {message: at for at, message in enumerate(RECEIVED)}


PRODUCTS = {"3_0": 3, "2": 1, "3_1": 2, "4_0": 2, "3_2": 2, "4_-1": 1, "4_1": 1}


class RingGather:
    def __init__(self, me, part, send, recv):
        self.z, self.x = me // SIDE, lax.rem(me, SIDE)
        self.part, self.send, self.recv = part, send, recv

    def slot(self, k, po, qo):
        dx, dz = (po, qo) if k == 0 else (qo, po)
        z = lax.rem(self.z + dz + SIDE, SIDE)
        x = lax.rem(self.x + dx + SIDE, SIDE)
        return z * SIDE + x

    def copy(self, ref, k, stage, po, d, to):
        sem = self.recv.at[INDEX[k, stage, po, 0 if stage in (2, 4) else d]]
        return pltpu.make_async_remote_copy(
            src_ref=ref,
            dst_ref=ref,
            send_sem=self.send,
            recv_sem=sem,
            device_id={"fs": to},
            device_id_type=MESH,
        )

    def start(self, k, stage, po, d):
        first = stage in (1, 2)
        at = {1: (0, 0), 2: (-d, 0), 3: (po, 0), 4: (po, -d)}[stage]
        half = None if stage in (1, 3) else (0 if d > 0 else 1)
        to = self.slot(k, d, 0) if first else self.slot(k, 0, d)
        ref = self.part(self.slot(k, *at), k, half)
        self.copy(ref, k, stage, po, d, to).start()

    def wait(self, k, stage, po, d=0):
        at = {1: (-d, 0), 2: (2, 0), 3: (po, -d), 4: (po, 2)}[stage]
        ref = self.part(self.slot(k, *at), k, None)
        with jax.named_scope(f"wait_{k}_{stage}_{po}_{d}"):
            self.copy(ref, k, stage, po, d, self.slot(k, 1, 0)).wait_recv()

    def run(self, arrived, after):
        for stage in (1, 3):
            for d in (1, -1):
                for k in (0, 1):
                    self.start(k, stage, 0, d)
        after("start")
        for d in (1, -1):
            for k in (0, 1):
                self.wait(k, 1, 0, d)
                self.start(k, 2, 0, d)
                self.start(k, 3, -d, 1)
                self.start(k, 3, -d, -1)
                arrived(k, -d, 0)
        self.second(arrived, 0)
        after("3_0")
        for k in (0, 1):
            self.wait(k, 2, 0)
            self.start(k, 3, 2, 1)
            self.start(k, 3, 2, -1)
            arrived(k, 2, 0)
        after("2")
        for po in (-1, 1):
            self.second(arrived, po)
            after(f"3_{po}")
        self.last(arrived, 0)
        after("4_0")
        self.second(arrived, 2)
        after("3_2")
        for po in (-1, 1, 2):
            self.last(arrived, po)
            after(f"4_{po}")

    def second(self, arrived, po):
        for d in (1, -1):
            for k in (0, 1):
                self.wait(k, 3, po, d)
                self.start(k, 4, po, d)
                arrived(k, po, -d)

    def last(self, arrived, po):
        for k in (0, 1):
            self.wait(k, 4, po)
            arrived(k, po, 2)

    def finish(self, everything):
        self.copy(everything, 0, 1, 0, 1, self.slot(0, 1, 0)).wait_send()


def high_low(values):
    upper = values.astype(BF16)
    return upper, (values - upper.astype(F32)).astype(BF16)


def kernel(
    inputs,
    value_cot,
    gate_cot,
    out_cot,
    conv_output,
    factors,
    value_weight,
    gate_weight,
    out_weight,
    first_moment,
    second_moment,
    mom,
    upd,
    copies,
    inp,
    oct_,
    cots,
    cots_t,
    fbuf,
    wbuf,
    summed,
    pieces,
    arrived,
    dirs,
    sums,
    fs_sums,
    load_sem,
    ring_send,
    ring_recv,
    core_send,
    core_recv,
    a_send,
    a_recv,
    d_send,
    d_recv,
    s_send,
    s_recv,
):
    me = lax.axis_index("fs")
    t = lax.axis_index("tp")
    core = lax.rem(t, 2)
    partner = t + 1 - 2 * core

    def load(at, *pairs):
        for src, dst in pairs:
            pltpu.make_async_copy(src, dst, load_sem.at[at]).start()

    def loaded(at, ref):
        pltpu.make_async_copy(ref, ref, load_sem.at[at]).wait()

    load(0, (factors, fbuf.at[me]))
    load(1, *((r, cots.at[m]) for m, r in enumerate((value_cot, gate_cot, conv_output))))
    load(2, (inputs, inp))
    load(3, (out_cot, oct_))
    load(4, (first_moment, mom.at[0]), (second_moment, mom.at[1]))
    load(5, *((r, wbuf.at[m]) for m, r in enumerate((value_weight, gate_weight, out_weight))))

    barrier = pltpu.get_barrier_semaphore()

    def greet_fs(j, _):
        pl.semaphore_signal(
            barrier, inc=1, device_id={"fs": lax.rem(me + j, FS)}, device_id_type=MESH
        )
        return _

    def greet_tp(j, _):
        pl.semaphore_signal(
            barrier, inc=1, device_id={"tp": lax.rem(t + j, TP)}, device_id_type=MESH
        )
        return _

    lax.fori_loop(1, FS, greet_fs, 0)
    lax.fori_loop(1, TP, greet_tp, 0)

    with jax.named_scope("turn"):
        loaded(1, cots)
        for m in range(3):

            def turn(i, _):
                rows = pl.ds(pl.multiple_of(i * 256, 256), 256)
                cots_t[m, :, rows] = cots[m, rows, :].T
                return _

            lax.fori_loop(0, TOK // 256, turn, 0)

    with jax.named_scope("barrier"):
        pl.semaphore_wait(barrier, FS - 1 + TP - 1)

    def factor_part(of_core):
        def part(s, k, half):
            at = of_core * 128 + 64 * k
            size = 64
            if half is not None:
                at, size = at + 32 * half, 32
            return fbuf.at[s, :, pl.ds(pl.multiple_of(at, 32), size), :]

        return part

    ring = RingGather(me, factor_part(core), ring_send.at[0], ring_recv)

    def core_copy(ref, dx, dz):
        return pltpu.make_async_remote_copy(
            src_ref=ref,
            dst_ref=ref,
            send_sem=core_send.at[0],
            recv_sem=core_recv.at[(dx + 1) * SIDE + dz + 1],
            device_id={"tp": partner},
            device_id_type=MESH,
        )

    def half_of(of_core, *slots):
        at = pl.multiple_of(of_core * 128, 128)
        return fbuf.at[(*slots, slice(None), pl.ds(at, 128), slice(None))]

    def multiply(s, first):
        cols = pl.ds(pl.multiple_of(s * W, W), W)

        def tile(i, _):
            rows = pl.ds(pl.multiple_of(i * 512, 512), 512)
            left = inp[rows, cols]
            other = oct_[rows, cols]
            for m in range(3):
                product = jnp.dot(
                    other if m == 2 else left, fbuf[s, m], preferred_element_type=F32
                )
                if first:
                    summed[m, rows, :] = product
                else:
                    summed[m, rows, :] += product
            return _

        with jax.named_scope("multiply"):
            lax.fori_loop(0, TOK // 512, tile, 0)

    loaded(0, fbuf.at[me])
    halves = set()
    waiting = []

    def multiply_next():
        dx, dz = waiting.pop(0)
        with jax.named_scope("wait_share"):
            s = ring.slot(0, dx, dz)
            core_copy(half_of(1 - core, s), dx, dz).wait_recv()
        multiply(s, False)

    def on_factor(k, po, qo):
        dx, dz = (po, qo) if k == 0 else (qo, po)
        core_copy(factor_part(core)(ring.slot(k, po, qo), k, None), dx, dz).start()
        if (dx, dz) in halves:
            waiting.append((dx, dz))
        halves.add((dx, dz))

    def between(group):
        if group == "start":
            with jax.named_scope("wait_loads"):
                loaded(2, inp)
                loaded(3, oct_)
            multiply(me, True)
        for _ in range(PRODUCTS.get(group, 0)):
            multiply_next()

    ring.run(on_factor, between)
    while waiting:
        multiply_next()

    def loop(start, stop, step):
        def body(j, carry):
            step(j)
            return carry

        lax.fori_loop(start, stop, body, 0)

    def to_fs(src, dst, send, recv, j):
        return pltpu.make_async_remote_copy(
            src_ref=src,
            dst_ref=dst,
            send_sem=send,
            recv_sem=recv,
            device_id={"fs": lax.rem(me + j, FS)},
            device_id_type=MESH,
        )

    others = pl.ds(0, FS - 1)

    for m in range(3):
        with jax.named_scope("project"):
            upper, lower = high_low(summed[m])
            product = jnp.dot(cots_t[m], upper, preferred_element_type=F32)
            product += jnp.dot(cots_t[m], lower, preferred_element_type=F32)
            pieces[m] = product.T.reshape(FS, RS, W)

        def send_piece(j):
            to_fs(
                pieces.at[m, lax.rem(me + j, FS)],
                arrived.at[m, me],
                a_send.at[0],
                a_recv.at[m],
                j,
            ).start()

        loop(1, FS, send_piece)
        arrived[m, me] = pieces[m, me]

    loaded(4, mom)
    squares = jnp.zeros((8, W), F32)
    for m in range(3):
        with jax.named_scope("wait_pieces"):
            ref = arrived.at[m, others]
            to_fs(ref, ref, a_send.at[0], a_recv.at[m], 1).wait_recv()
        projected = jnp.sum(arrived[m], axis=0)
        new_first = FIRST_DECAY * mom[0, m] + (1.0 - FIRST_DECAY) * projected
        new_second = (
            SECOND_DECAY * mom[1, m] + (1.0 - SECOND_DECAY) * projected * projected
        )
        direction = new_first / (jnp.sqrt(new_second) + DIVISOR_EPS)
        mom[0, m] = new_first
        mom[1, m] = new_second
        dirs[m, me] = direction

        def send_direction(j):
            ref = dirs.at[m, me]
            to_fs(ref, ref, d_send.at[0], d_recv.at[m], j).start()

        loop(1, FS, send_direction)
        squares += direction[:8] * direction[:8] + direction[8:] * direction[8:]

    sums[t] = squares[:, :128] + squares[:, 128:]

    def to_tp(ref, j):
        return pltpu.make_async_remote_copy(
            src_ref=ref,
            dst_ref=ref,
            send_sem=s_send.at[0],
            recv_sem=s_recv.at[0],
            device_id={"tp": lax.rem(t + j, TP)},
            device_id_type=MESH,
        )

    loop(1, TP, lambda j: to_tp(sums.at[t], j).start())

    def update(m):
        with jax.named_scope("wait_directions"):
            ref = dirs.at[m, others]
            to_fs(ref, ref, d_send.at[0], d_recv.at[m], 1).wait_recv()
        whole = dirs[m].reshape(RANK, W)
        if m == 2:
            upper, lower = high_low(whole.T)
            contract = (((1,), (1,)), ((), ()))
            own = fbuf[me, m]
            product = lax.dot_general(upper, own, contract, preferred_element_type=F32)
            product += lax.dot_general(lower, own, contract, preferred_element_type=F32)
        else:
            upper, lower = high_low(whole)
            product = jnp.dot(fbuf[me, m], upper, preferred_element_type=F32)
            product += jnp.dot(fbuf[me, m], lower, preferred_element_type=F32)
        upd[m] = product

    update(0)
    with jax.named_scope("wait_scalar"):
        to_tp(sums.at[pl.ds(0, TP - 1)], 1).wait_recv()
    fs_sums[me] = jnp.sum(sums[...], axis=0)

    def send_sum(j):
        ref = fs_sums.at[me]
        to_fs(ref, ref, s_send.at[1], s_recv.at[1], j).start()

    loop(1, FS, send_sum)
    update(1)
    loaded(5, wbuf)
    ring.finish(half_of(0, others))
    update(2)
    with jax.named_scope("wait_fs_scalar"):
        ref = fs_sums.at[others]
        to_fs(ref, ref, s_send.at[1], s_recv.at[1], 1).wait_recv()
    total = jnp.sum(jnp.sum(fs_sums[...], axis=0), keepdims=True)
    norm_scale = lax.rsqrt(total / (3 * RANK * C) + SQUARE_EPS)
    for m in range(3):
        scaled = norm_scale * upd[m]
        upd[m] = scaled
        copies[me, m] = (wbuf[m] - LEARN_RATE * scaled).astype(BF16)

    def copy_part(s, k, half):
        at, size = 128 * k, 128
        if half is not None:
            at, size = at + 64 * half, 64
        return copies.at[s, :, pl.ds(at, size), :]

    gather = RingGather(me, copy_part, ring_send.at[0], ring_recv)
    gather.run(lambda k, po, qo: None, lambda group: None)

    with jax.named_scope("finish"):
        gather.finish(copies.at[others])
        core_copy(half_of(0, others), 0, 0).wait_send()
        for m in range(3):
            ref = pieces.at[m, others]
            to_fs(ref, ref, a_send.at[0], a_recv.at[m], 1).wait_send()
            ref = dirs.at[m, others]
            to_fs(ref, ref, d_send.at[0], d_recv.at[m], 1).wait_send()
        to_tp(sums.at[pl.ds(0, TP - 1)], 1).wait_send()
        ref = fs_sums.at[others]
        to_fs(ref, ref, s_send.at[1], s_recv.at[1], 1).wait_send()


def store_kernel(
    mom,
    upd,
    copies,
    first_out,
    second_out,
    value_update,
    gate_update,
    out_update,
    value_copy,
    gate_copy,
    out_copy,
    sem,
):
    def store(src, dst):
        pltpu.make_async_copy(src, dst, sem.at[0]).start()

    def store_block(s, carry):
        at = pl.ds(pl.multiple_of(s * W, W), W)
        store(copies.at[s, 0], value_copy.at[at, :])
        store(copies.at[s, 1], gate_copy.at[at, :])
        store(copies.at[s, 2], out_copy.at[:, at])
        return carry

    lax.fori_loop(0, FS, store_block, 0)
    store(upd.at[0], value_update)
    store(upd.at[1], gate_update)
    store(upd.at[2], out_update)
    store(mom.at[0], first_out)
    store(mom.at[1], second_out)
    for ref in (copies, upd, mom):
        pltpu.make_async_copy(ref, ref, sem.at[0]).wait()


def shards(*args):
    anywhere = pl.BlockSpec(memory_space=pl.ANY)
    vmem = pl.BlockSpec(memory_space=pltpu.VMEM)
    dma = pltpu.SemaphoreType.DMA
    results = pl.pallas_call(
        kernel,
        out_shape=(
            pltpu.VMEM((2, 3, RS, W), F32),
            pltpu.VMEM((3, W, W), F32),
            pltpu.VMEM((FS, 3, W, W), BF16),
        ),
        in_specs=[anywhere] * 11,
        out_specs=(vmem,) * 3,
        scratch_shapes=[
            pltpu.VMEM((TOK, D), BF16),
            pltpu.VMEM((TOK, D), BF16),
            pltpu.VMEM((3, TOK, W), BF16),
            pltpu.VMEM((3, W, TOK), BF16),
            pltpu.VMEM((FS, 3, W, RANK), BF16),
            pltpu.VMEM((3, W, W), F32),
            pltpu.VMEM((3, TOK, RANK), F32),
            pltpu.VMEM((3, FS, RS, W), F32),
            pltpu.VMEM((3, FS, RS, W), F32),
            pltpu.VMEM((3, FS, RS, W), F32),
            pltpu.VMEM((TP, 8, 128), F32),
            pltpu.VMEM((FS, 8, 128), F32),
            dma((6,)),
            dma((1,)),
            dma((len(RECEIVED),)),
            dma((1,)),
            dma((FS,)),
            dma((1,)),
            dma((3,)),
            dma((1,)),
            dma((3,)),
            dma((2,)),
            dma((2,)),
        ],
        compiler_params=pltpu.CompilerParams(
            collective_id=0, has_side_effects=True, vmem_limit_bytes=48 * 1024 * 1024
        ),
    )(*[pltpu.with_memory_space_constraint(a, pltpu.HBM) for a in args])
    return pl.pallas_call(
        store_kernel,
        out_shape=(
            jax.ShapeDtypeStruct((3, RS, W), F32),
            jax.ShapeDtypeStruct((3, RS, W), F32),
            jax.ShapeDtypeStruct((W, W), F32),
            jax.ShapeDtypeStruct((W, W), F32),
            jax.ShapeDtypeStruct((W, W), F32),
            jax.ShapeDtypeStruct((D, W), BF16),
            jax.ShapeDtypeStruct((D, W), BF16),
            jax.ShapeDtypeStruct((W, D), BF16),
        ),
        in_specs=[vmem] * 3,
        out_specs=(anywhere,) * 8,
        scratch_shapes=[dma((1,))],
        compiler_params=pltpu.CompilerParams(vmem_limit_bytes=4 * 1024 * 1024),
    )(*[pltpu.with_memory_space_constraint(r, pltpu.VMEM) for r in results])


def solution(mesh):
    placed = (
        P("fs", None),
        P("fs", "tp"),
        P("fs", "tp"),
        P("fs", None),
        P("fs", "tp"),
        P(None, "fs", None),
        P("fs", "tp"),
        P("fs", "tp"),
        P("tp", "fs"),
        P(None, "fs", "tp"),
        P(None, "fs", "tp"),
    )
    return jax.shard_map(
        shards,
        mesh=mesh,
        in_specs=placed,
        out_specs=(
            P(None, "fs", "tp"),
            P(None, "fs", "tp"),
            P("fs", "tp"),
            P("fs", "tp"),
            P("tp", "fs"),
            P(None, "tp"),
            P(None, "tp"),
            P("tp", None),
        ),
        check_vma=False,
    )
```

time: 99.1 us -> 92 us (0.928)
  Pallas kernels: 98.3 us -> 91 us
    pallas_call x1, Pallas kernels: 95 us -> 88.1 us  [shards(): pl.pallas_call(kernel, out_shape=(pltpu.VMEM((2, 3, RS, W), F32), pltpu.V...]
where the time goes in v3:
time: 92 us; the launch traced here: 91.6 us
  Pallas kernels  91 us (99%)
    pallas_call x1, Pallas kernels, shards(): pl.pallas_call(kernel, out_shape=(pltpu.VMEM((2, 3, RS, W), F32), pltpu.V...  88.1 us
    pallas_call x1, Pallas kernels, shards(): pl.pallas_call(store_kernel, out_shape=(jax.ShapeDtypeStruct((3, RS, W),...  2.87 us

profile of v3, /device:TPU:0, one launch (start us, length us, event | category | flops | bytes accessed | tf_op | source)
XLA Modules:
  0.0 91.6 jit_solution(2807948030245334822)
XLA Ops:
  0.6 88.1 %shard_map.170 = (f32[2,3,16,256]{3,2,1,0:T(8,128)S(1)}, f32[3,256,256]{2,1,0:T(8,128)S(1)}, bf16[16,3,256,256]{3,2,1,0:T(8,128)(2,1)S(1)}) custom-call(bf16[1024,4096]{1,0:T(8,128)(2,1)} %inputs.1, bf16[1024,256]{1,0:T(8,128)(2,1)} %value_cot.1, bf16[1024,256]{1,0:T(8,128)(2,1)} %gate_cot.1, bf16[1024,4096]{1,0:T(8,128)(2,1)} %out_cot.1, ...), custom_call_target="tpu_custom_call" | custom-call | tf_op jit(solution)/shard_map/pallas_call | solution.py:471
  88.7 2.9 %shard_map.171 = (f32[3,16,256]{2,1,0:T(8,128)}, f32[3,16,256]{2,1,0:T(8,128)}, f32[256,256]{1,0:T(8,128)}, f32[256,256]{1,0:T(8,128)}, f32[256,256]{1,0:T(8,128...) custom-call(f32[2,3,16,256]{3,2,1,0:T(8,128)S(1)} %get-tuple-element.11.mom, ...), custom_call_target="tpu_custom_call" | custom-call | tf_op jit(solution)/shard_map/pallas_call | solution.py:509

commit v4 on v3

--- a/solution.py
+++ b/solution.py
@@ -18,6 +18,7 @@
 SIDE = 4
 FS = SIDE * SIDE
 TP = 8
+HALF = 128
 W = 256
 RS = RANK // FS
 TOK = 1024
@@ -34,11 +35,9 @@
 INDEX = {message: at for at, message in enumerate(RECEIVED)}
 
 
-PRODUCTS = {"3_0": 3, "2": 1, "3_1": 2, "4_0": 2, "3_2": 2, "4_-1": 1, "4_1": 1}
-
-
 class RingGather:
-    def __init__(self, me, part, send, recv):
+    def __init__(self, name, me, part, send, recv):
+        self.name = name
         self.z, self.x = me // SIDE, lax.rem(me, SIDE)
         self.part, self.send, self.recv = part, send, recv
 
@@ -70,40 +69,43 @@
     def wait(self, k, stage, po, d=0):
         at = {1: (-d, 0), 2: (2, 0), 3: (po, -d), 4: (po, 2)}[stage]
         ref = self.part(self.slot(k, *at), k, None)
-        with jax.named_scope(f"wait_{k}_{stage}_{po}_{d}"):
+        with jax.named_scope(f"w{self.name}_{k}_{stage}_{po}_{d}"):
             self.copy(ref, k, stage, po, d, self.slot(k, 1, 0)).wait_recv()
 
-    def run(self, arrived, after):
+    def steps(self, arrived):
         for stage in (1, 3):
             for d in (1, -1):
                 for k in (0, 1):
                     self.start(k, stage, 0, d)
-        after("start")
+        yield "start"
         for d in (1, -1):
             for k in (0, 1):
                 self.wait(k, 1, 0, d)
                 self.start(k, 2, 0, d)
-                self.start(k, 3, -d, 1)
-                self.start(k, 3, -d, -1)
                 arrived(k, -d, 0)
+        for po in (-1, 1):
+            for d in (1, -1):
+                for k in (0, 1):
+                    self.start(k, 3, po, d)
+        yield "1"
         self.second(arrived, 0)
-        after("3_0")
+        yield "3_0"
         for k in (0, 1):
             self.wait(k, 2, 0)
             self.start(k, 3, 2, 1)
             self.start(k, 3, 2, -1)
             arrived(k, 2, 0)
-        after("2")
+        yield "2"
         for po in (-1, 1):
             self.second(arrived, po)
-            after(f"3_{po}")
+            yield f"3_{po}"
         self.last(arrived, 0)
-        after("4_0")
+        yield "4_0"
         self.second(arrived, 2)
-        after("3_2")
+        yield "3_2"
         for po in (-1, 1, 2):
             self.last(arrived, po)
-            after(f"4_{po}")
+            yield f"4_{po}"
 
     def second(self, arrived, po):
         for d in (1, -1):
@@ -141,14 +143,15 @@
     mom,
     upd,
     copies,
-    inp,
-    oct_,
+    left,
     cots,
     cots_t,
     fbuf,
+    fown,
     wbuf,
     summed,
     pieces,
+    from_core,
     arrived,
     dirs,
     sums,
@@ -177,12 +180,21 @@
     def loaded(at, ref):
         pltpu.make_async_copy(ref, ref, load_sem.at[at]).wait()
 
-    load(0, (factors, fbuf.at[me]))
+    half = pl.ds(pl.multiple_of(core * HALF, HALF), HALF)
+    load(0, (factors.at[:, half, :], fbuf.at[me]))
     load(1, *((r, cots.at[m]) for m, r in enumerate((value_cot, gate_cot, conv_output))))
-    load(2, (inputs, inp))
-    load(3, (out_cot, oct_))
+
+    def load_half(s, carry):
+        src = pl.ds(pl.multiple_of(s * W + core * HALF, HALF), HALF)
+        dst = pl.ds(pl.multiple_of(s * HALF, HALF), HALF)
+        load(2, (inputs.at[:, src], left.at[0, :, dst]))
+        load(3, (out_cot.at[:, src], left.at[1, :, dst]))
+        return carry
+
+    lax.fori_loop(0, FS, load_half, 0)
     load(4, (first_moment, mom.at[0]), (second_moment, mom.at[1]))
     load(5, *((r, wbuf.at[m]) for m, r in enumerate((value_weight, gate_weight, out_weight))))
+    load(6, (factors, fown))
 
     barrier = pltpu.get_barrier_semaphore()
 
@@ -207,7 +219,7 @@
 
             def turn(i, _):
                 rows = pl.ds(pl.multiple_of(i * 256, 256), 256)
-                cots_t[m, :, rows] = cots[m, rows, :].T
+                cots_t[0, m, :, rows] = cots[m, rows, :].T
                 return _
 
             lax.fori_loop(0, TOK // 256, turn, 0)
@@ -215,82 +227,76 @@
     with jax.named_scope("barrier"):
         pl.semaphore_wait(barrier, FS - 1 + TP - 1)
 
-    def factor_part(of_core):
-        def part(s, k, half):
-            at = of_core * 128 + 64 * k
-            size = 64
-            if half is not None:
-                at, size = at + 32 * half, 32
-            return fbuf.at[s, :, pl.ds(pl.multiple_of(at, 32), size), :]
-
-        return part
-
-    ring = RingGather(me, factor_part(core), ring_send.at[0], ring_recv)
-
-    def core_copy(ref, dx, dz):
+    def to_partner(src, dst, at):
+        return pltpu.make_async_remote_copy(
+            src_ref=src,
+            dst_ref=dst,
+            send_sem=core_send.at[0],
+            recv_sem=core_recv.at[at],
+            device_id={"tp": partner},
+            device_id_type=MESH,
+        )
+
+    def factor_part(s, k, half):
+        at, size = 64 * k, 64
+        if half is not None:
+            at, size = at + 32 * half, 32
+        return fbuf.at[s, pl.ds(odd_base, 2), pl.ds(at, size), :]
+
+    y = t // 2
+    odd = lax.rem(y, 2)
+    odd_base = 1 - odd
+    lacking, handed = 2 * odd, 2 - 2 * odd
+
+    def along_y(ref, k):
         return pltpu.make_async_remote_copy(
             src_ref=ref,
             dst_ref=ref,
-            send_sem=core_send.at[0],
-            recv_sem=core_recv.at[(dx + 1) * SIDE + dz + 1],
-            device_id={"tp": partner},
+            send_sem=core_send.at[1],
+            recv_sem=core_recv.at[4],
+            device_id={"tp": lax.rem(t + (2 if k == 0 else TP - 2), TP)},
             device_id_type=MESH,
         )
 
-    def half_of(of_core, *slots):
-        at = pl.multiple_of(of_core * 128, 128)
-        return fbuf.at[(*slots, slice(None), pl.ds(at, 128), slice(None))]
-
-    def multiply(s, first):
-        cols = pl.ds(pl.multiple_of(s * W, W), W)
-
-        def tile(i, _):
-            rows = pl.ds(pl.multiple_of(i * 512, 512), 512)
-            left = inp[rows, cols]
-            other = oct_[rows, cols]
-            for m in range(3):
+    ring = RingGather("a", me, factor_part, ring_send.at[0], ring_recv)
+    parts_here, waiting = set(), []
+
+    def factor_arrived(k, po, qo):
+        dx, dz = (po, qo) if k == 0 else (qo, po)
+        s = ring.slot(0, dx, dz)
+        along_y(fbuf.at[s, handed, pl.ds(64 * k, 64), :], k).start()
+        if (dx, dz) in parts_here:
+            waiting.append(s)
+        parts_here.add((dx, dz))
+
+    def multiply(*slots, first=False):
+        with jax.named_scope("multiply"):
+            for m in (odd_base, odd_base + 1):
+                ours = [
+                    left[m // 2, :, pl.ds(pl.multiple_of(s * HALF, HALF), HALF)]
+                    for s in slots
+                ]
                 product = jnp.dot(
-                    other if m == 2 else left, fbuf[s, m], preferred_element_type=F32
+                    jnp.concatenate(ours, axis=1),
+                    jnp.concatenate([fbuf[s, m] for s in slots], axis=0),
+                    preferred_element_type=F32,
                 )
                 if first:
-                    summed[m, rows, :] = product
+                    summed[m] = product
                 else:
-                    summed[m, rows, :] += product
-            return _
-
-        with jax.named_scope("multiply"):
-            lax.fori_loop(0, TOK // 512, tile, 0)
-
-    loaded(0, fbuf.at[me])
-    halves = set()
-    waiting = []
-
-    def multiply_next():
-        dx, dz = waiting.pop(0)
-        with jax.named_scope("wait_share"):
-            s = ring.slot(0, dx, dz)
-            core_copy(half_of(1 - core, s), dx, dz).wait_recv()
-        multiply(s, False)
-
-    def on_factor(k, po, qo):
-        dx, dz = (po, qo) if k == 0 else (qo, po)
-        core_copy(factor_part(core)(ring.slot(k, po, qo), k, None), dx, dz).start()
-        if (dx, dz) in halves:
-            waiting.append((dx, dz))
-        halves.add((dx, dz))
-
-    def between(group):
-        if group == "start":
-            with jax.named_scope("wait_loads"):
-                loaded(2, inp)
-                loaded(3, oct_)
-            multiply(me, True)
-        for _ in range(PRODUCTS.get(group, 0)):
-            multiply_next()
-
-    ring.run(on_factor, between)
-    while waiting:
-        multiply_next()
+                    summed[m] += product
+
+    def multiply_lacking():
+        with jax.named_scope("multiply_lacking"):
+            right = fbuf[:, lacking].reshape(D // 2, RANK)
+
+            def tile(i, carry):
+                rows = pl.ds(pl.multiple_of(i * 256, 256), 256)
+                ours = left[lacking // 2, rows, :]
+                summed[lacking, rows, :] = jnp.dot(ours, right, preferred_element_type=F32)
+                return carry
+
+            lax.fori_loop(0, TOK // 256, tile, 0)
 
     def loop(start, stop, step):
         def body(j, carry):
@@ -311,16 +317,24 @@
 
     others = pl.ds(0, FS - 1)
 
-    for m in range(3):
+    def project(m):
         with jax.named_scope("project"):
-            upper, lower = high_low(summed[m])
-            product = jnp.dot(cots_t[m], upper, preferred_element_type=F32)
-            product += jnp.dot(cots_t[m], lower, preferred_element_type=F32)
-            pieces[m] = product.T.reshape(FS, RS, W)
+            split = jnp.concatenate(high_low(summed[m]), axis=1)
+            turned = cots_t[:, m].reshape(2 * W, TOK)
+            product = jnp.dot(turned, split, preferred_element_type=F32)
+            product = product[:, :RANK] + product[:, RANK:]
+            pieces[1, m] = product[W:].T.reshape(FS, RS, W)
+            to_partner(pieces.at[1, m], from_core.at[m], m).start()
+            pieces[0, m] = product[:W].T.reshape(FS, RS, W)
+
+    def send_pieces(m):
+        with jax.named_scope("wait_core"):
+            to_partner(pieces.at[1, m], from_core.at[m], m).wait_recv()
+        pieces[0, m] += from_core[m]
 
         def send_piece(j):
             to_fs(
-                pieces.at[m, lax.rem(me + j, FS)],
+                pieces.at[0, m, lax.rem(me + j, FS)],
                 arrived.at[m, me],
                 a_send.at[0],
                 a_recv.at[m],
@@ -328,11 +342,11 @@
             ).start()
 
         loop(1, FS, send_piece)
-        arrived[m, me] = pieces[m, me]
-
-    loaded(4, mom)
-    squares = jnp.zeros((8, W), F32)
-    for m in range(3):
+        arrived[m, me] = pieces[0, m, me]
+
+    squares = []
+
+    def moments(m):
         with jax.named_scope("wait_pieces"):
             ref = arrived.at[m, others]
             to_fs(ref, ref, a_send.at[0], a_recv.at[m], 1).wait_recv()
@@ -351,9 +365,42 @@
             to_fs(ref, ref, d_send.at[0], d_recv.at[m], j).start()
 
         loop(1, FS, send_direction)
-        squares += direction[:8] * direction[:8] + direction[8:] * direction[8:]
-
-    sums[t] = squares[:, :128] + squares[:, 128:]
+        squares.append(direction[:8] * direction[:8] + direction[8:] * direction[8:])
+
+    loaded(0, fbuf.at[me])
+    groups = ring.steps(factor_arrived)
+
+    def to(group):
+        while next(groups) != group:
+            pass
+
+    to("start")
+    to_partner(cots_t.at[0], cots_t.at[1], 3).start()
+    with jax.named_scope("wait_loads"):
+        loaded(2, left.at[0])
+        loaded(3, left.at[1])
+    multiply(me, first=True)
+    for group in ("2", "4_0", "4_-1", "4_2"):
+        to(group)
+        multiply(*waiting)
+        waiting.clear()
+    to_partner(cots_t.at[0], cots_t.at[1], 3).wait_recv()
+    order = (odd_base, odd_base + 1, lacking)
+    project(order[0])
+    project(order[1])
+    send_pieces(order[0])
+    with jax.named_scope("wait_y"):
+        along_y(fbuf.at[others, 0], 0).wait_recv()
+    multiply_lacking()
+    send_pieces(order[1])
+    project(order[2])
+    send_pieces(order[2])
+    loaded(4, mom)
+    for m in order:
+        moments(m)
+
+    square = squares[0] + squares[1] + squares[2]
+    sums[t] = square[:, :128] + square[:, 128:]
 
     def to_tp(ref, j):
         return pltpu.make_async_remote_copy(
@@ -367,24 +414,28 @@
 
     loop(1, TP, lambda j: to_tp(sums.at[t], j).start())
 
-    def update(m):
+    def wait_directions(m):
         with jax.named_scope("wait_directions"):
             ref = dirs.at[m, others]
             to_fs(ref, ref, d_send.at[0], d_recv.at[m], 1).wait_recv()
-        whole = dirs[m].reshape(RANK, W)
+
+    def update(m):
+        full = dirs[m].reshape(RANK, W)
         if m == 2:
-            upper, lower = high_low(whole.T)
+            upper, lower = high_low(full.T)
             contract = (((1,), (1,)), ((), ()))
-            own = fbuf[me, m]
+            own = fown[m]
             product = lax.dot_general(upper, own, contract, preferred_element_type=F32)
             product += lax.dot_general(lower, own, contract, preferred_element_type=F32)
         else:
-            upper, lower = high_low(whole)
-            product = jnp.dot(fbuf[me, m], upper, preferred_element_type=F32)
-            product += jnp.dot(fbuf[me, m], lower, preferred_element_type=F32)
+            upper, lower = high_low(full)
+            product = jnp.dot(fown[m], upper, preferred_element_type=F32)
+            product += jnp.dot(fown[m], lower, preferred_element_type=F32)
         upd[m] = product
 
-    update(0)
+    loaded(6, fown)
+    loaded(5, wbuf)
+    wait_directions(order[0])
     with jax.named_scope("wait_scalar"):
         to_tp(sums.at[pl.ds(0, TP - 1)], 1).wait_recv()
     fs_sums[me] = jnp.sum(sums[...], axis=0)
@@ -394,9 +445,12 @@
         to_fs(ref, ref, s_send.at[1], s_recv.at[1], j).start()
 
     loop(1, FS, send_sum)
+    wait_directions(order[1])
     update(1)
-    loaded(5, wbuf)
-    ring.finish(half_of(0, others))
+    ring.finish(fbuf.at[others, pl.ds(0, 2)])
+    along_y(fbuf.at[others, 0], 0).wait_send()
+    wait_directions(order[2])
+    update(0)
     update(2)
     with jax.named_scope("wait_fs_scalar"):
         ref = fs_sums.at[others]
@@ -414,14 +468,16 @@
             at, size = at + 64 * half, 64
         return copies.at[s, :, pl.ds(at, size), :]
 
-    gather = RingGather(me, copy_part, ring_send.at[0], ring_recv)
-    gather.run(lambda k, po, qo: None, lambda group: None)
+    gather = RingGather("c", me, copy_part, ring_send.at[0], ring_recv)
+    for _ in gather.steps(lambda k, po, qo: None):
+        pass
 
     with jax.named_scope("finish"):
         gather.finish(copies.at[others])
-        core_copy(half_of(0, others), 0, 0).wait_send()
+        to_partner(cots_t.at[0], cots_t.at[1], 3).wait_send()
         for m in range(3):
-            ref = pieces.at[m, others]
+            to_partner(pieces.at[1, m], from_core.at[m], m).wait_send()
+            ref = pieces.at[0, m, others]
             to_fs(ref, ref, a_send.at[0], a_recv.at[m], 1).wait_send()
             ref = dirs.at[m, others]
             to_fs(ref, ref, d_send.at[0], d_recv.at[m], 1).wait_send()
@@ -478,23 +534,24 @@
         in_specs=[anywhere] * 11,
         out_specs=(vmem,) * 3,
         scratch_shapes=[
-            pltpu.VMEM((TOK, D), BF16),
-            pltpu.VMEM((TOK, D), BF16),
+            pltpu.VMEM((2, TOK, D // 2), BF16),
             pltpu.VMEM((3, TOK, W), BF16),
-            pltpu.VMEM((3, W, TOK), BF16),
-            pltpu.VMEM((FS, 3, W, RANK), BF16),
+            pltpu.VMEM((2, 3, W, TOK), BF16),
+            pltpu.VMEM((FS, 3, HALF, RANK), BF16),
+            pltpu.VMEM((3, W, RANK), BF16),
             pltpu.VMEM((3, W, W), F32),
             pltpu.VMEM((3, TOK, RANK), F32),
+            pltpu.VMEM((2, 3, FS, RS, W), F32),
             pltpu.VMEM((3, FS, RS, W), F32),
             pltpu.VMEM((3, FS, RS, W), F32),
             pltpu.VMEM((3, FS, RS, W), F32),
             pltpu.VMEM((TP, 8, 128), F32),
             pltpu.VMEM((FS, 8, 128), F32),
-            dma((6,)),
+            dma((7,)),
             dma((1,)),
             dma((len(RECEIVED),)),
-            dma((1,)),
-            dma((FS,)),
+            dma((2,)),
+            dma((5,)),
             dma((1,)),
             dma((3,)),
             dma((1,)),

time: 92 us -> 87.1 us (0.947)
  Pallas kernels: 91 us -> 86.4 us
    pallas_call x1, Pallas kernels: 88.1 us -> 83.5 us  [shards(): pl.pallas_call(kernel, out_shape=(pltpu.VMEM((2, 3, RS, W), F32), pltpu.V...]
where the time goes in v4:
time: 87.1 us; the launch traced here: 87 us
  Pallas kernels  86.4 us (99%)
    pallas_call x1, Pallas kernels, shards(): pl.pallas_call(kernel, out_shape=(pltpu.VMEM((2, 3, RS, W), F32), pltpu.V...  83.5 us
    pallas_call x1, Pallas kernels, shards(): pl.pallas_call(store_kernel, out_shape=(jax.ShapeDtypeStruct((3, RS, W),...  2.87 us

profile of v4, /device:TPU:0, one launch (start us, length us, event | category | flops | bytes accessed | tf_op | source)
XLA Modules:
  0.0 87.0 jit_solution(4953687094741540508)
XLA Ops:
  0.6 83.5 %shard_map.170 = (f32[2,3,16,256]{3,2,1,0:T(8,128)S(1)}, f32[3,256,256]{2,1,0:T(8,128)S(1)}, bf16[16,3,256,256]{3,2,1,0:T(8,128)(2,1)S(1)}) custom-call(bf16[1024,4096]{1,0:T(8,128)(2,1)} %inputs.1, bf16[1024,256]{1,0:T(8,128)(2,1)} %value_cot.1, bf16[1024,256]{1,0:T(8,128)(2,1)} %gate_cot.1, bf16[1024,4096]{1,0:T(8,128)(2,1)} %out_cot.1, ...), custom_call_target="tpu_custom_call" | custom-call | tf_op jit(solution)/shard_map/pallas_call | solution.py:527
  84.1 2.9 %shard_map.171 = (f32[3,16,256]{2,1,0:T(8,128)}, f32[3,16,256]{2,1,0:T(8,128)}, f32[256,256]{1,0:T(8,128)}, f32[256,256]{1,0:T(8,128)}, f32[256,256]{1,0:T(8,128...) custom-call(f32[2,3,16,256]{3,2,1,0:T(8,128)S(1)} %get-tuple-element.11.mom, ...), custom_call_target="tpu_custom_call" | custom-call | tf_op jit(solution)/shard_map/pallas_call | solution.py:566

commit v5 on v4

--- a/solution.py
+++ b/solution.py
@@ -147,7 +147,6 @@
     cots,
     cots_t,
     fbuf,
-    fown,
     wbuf,
     summed,
     pieces,
@@ -161,6 +160,7 @@
     ring_recv,
     core_send,
     core_recv,
+    batch_recv,
     a_send,
     a_recv,
     d_send,
@@ -181,7 +181,7 @@
         pltpu.make_async_copy(ref, ref, load_sem.at[at]).wait()
 
     half = pl.ds(pl.multiple_of(core * HALF, HALF), HALF)
-    load(0, (factors.at[:, half, :], fbuf.at[me]))
+    load(0, (factors, fbuf.at[me]))
     load(1, *((r, cots.at[m]) for m, r in enumerate((value_cot, gate_cot, conv_output))))
 
     def load_half(s, carry):
@@ -194,7 +194,6 @@
     lax.fori_loop(0, FS, load_half, 0)
     load(4, (first_moment, mom.at[0]), (second_moment, mom.at[1]))
     load(5, *((r, wbuf.at[m]) for m, r in enumerate((value_weight, gate_weight, out_weight))))
-    load(6, (factors, fown))
 
     barrier = pltpu.get_barrier_semaphore()
 
@@ -212,17 +211,6 @@
 
     lax.fori_loop(1, FS, greet_fs, 0)
     lax.fori_loop(1, TP, greet_tp, 0)
-
-    with jax.named_scope("turn"):
-        loaded(1, cots)
-        for m in range(3):
-
-            def turn(i, _):
-                rows = pl.ds(pl.multiple_of(i * 256, 256), 256)
-                cots_t[0, m, :, rows] = cots[m, rows, :].T
-                return _
-
-            lax.fori_loop(0, TOK // 256, turn, 0)
 
     with jax.named_scope("barrier"):
         pl.semaphore_wait(barrier, FS - 1 + TP - 1)
@@ -238,9 +226,9 @@
         )
 
     def factor_part(s, k, half):
-        at, size = 64 * k, 64
+        at, size = HALF * k, HALF
         if half is not None:
-            at, size = at + 32 * half, 32
+            at, size = at + 64 * half, 64
         return fbuf.at[s, pl.ds(odd_base, 2), pl.ds(at, size), :]
 
     y = t // 2
@@ -249,36 +237,71 @@
     lacking, handed = 2 * odd, 2 - 2 * odd
 
     def along_y(ref, k):
+        to = lax.rem(2 * y + (2 if k == 0 else TP - 2), TP) + k
         return pltpu.make_async_remote_copy(
             src_ref=ref,
             dst_ref=ref,
             send_sem=core_send.at[1],
             recv_sem=core_recv.at[4],
-            device_id={"tp": lax.rem(t + (2 if k == 0 else TP - 2), TP)},
+            device_id={"tp": to},
             device_id_type=MESH,
         )
 
     ring = RingGather("a", me, factor_part, ring_send.at[0], ring_recv)
-    parts_here, waiting = set(), []
+    here = []
+
+    def to_other_core(ref, batch):
+        return pltpu.make_async_remote_copy(
+            src_ref=ref,
+            dst_ref=ref,
+            send_sem=core_send.at[2],
+            recv_sem=batch_recv.at[batch],
+            device_id={"tp": partner},
+            device_id_type=MESH,
+        )
 
     def factor_arrived(k, po, qo):
-        dx, dz = (po, qo) if k == 0 else (qo, po)
-        s = ring.slot(0, dx, dz)
-        along_y(fbuf.at[s, handed, pl.ds(64 * k, 64), :], k).start()
-        if (dx, dz) in parts_here:
-            waiting.append(s)
-        parts_here.add((dx, dz))
-
-    def multiply(*slots, first=False):
+        s = ring.slot(k, po, qo)
+        if k == 0:
+            here.append((po, qo))
+            to_other_core(factor_part(s, 0, None), state["batch"]).start()
+        along_y(fbuf.at[s, handed, pl.ds(HALF * k, HALF), :], k).start()
+
+    state = {"batch": 0}
+    groups = ring.steps(factor_arrived)
+
+    def slots_until(group):
+        @pl.when(core == 1)
+        def _():
+            while next(groups) != group:
+                pass
+
+        count = len(here)
+
+        @pl.when(core == 0)
+        def _():
+            with jax.named_scope("wait_batch"):
+                ref = fbuf.at[pl.ds(0, count), pl.ds(0, 2), pl.ds(0, HALF), :]
+                to_other_core(ref, state["batch"]).wait_recv()
+
+        slots = []
+        for po, qo in here:
+            zero, one = ring.slot(0, po, qo), ring.slot(1, po, qo)
+            slots.append(zero + core * (one - zero))
+        here.clear()
+        state["batch"] += 1
+        return slots
+
+    def multiply(*slots, first=False, matrices=(odd_base, odd_base + 1)):
         with jax.named_scope("multiply"):
-            for m in (odd_base, odd_base + 1):
+            for m in matrices:
                 ours = [
                     left[m // 2, :, pl.ds(pl.multiple_of(s * HALF, HALF), HALF)]
                     for s in slots
                 ]
                 product = jnp.dot(
                     jnp.concatenate(ours, axis=1),
-                    jnp.concatenate([fbuf[s, m] for s in slots], axis=0),
+                    jnp.concatenate([fbuf[s, m, half, :] for s in slots], axis=0),
                     preferred_element_type=F32,
                 )
                 if first:
@@ -288,7 +311,7 @@
 
     def multiply_lacking():
         with jax.named_scope("multiply_lacking"):
-            right = fbuf[:, lacking].reshape(D // 2, RANK)
+            right = fbuf[:, lacking, half, :].reshape(D // 2, RANK)
 
             def tile(i, carry):
                 rows = pl.ds(pl.multiple_of(i * 256, 256), 256)
@@ -320,12 +343,12 @@
     def project(m):
         with jax.named_scope("project"):
             split = jnp.concatenate(high_low(summed[m]), axis=1)
-            turned = cots_t[:, m].reshape(2 * W, TOK)
-            product = jnp.dot(turned, split, preferred_element_type=F32)
-            product = product[:, :RANK] + product[:, RANK:]
-            pieces[1, m] = product[W:].T.reshape(FS, RS, W)
-            to_partner(pieces.at[1, m], from_core.at[m], m).start()
-            pieces[0, m] = product[:W].T.reshape(FS, RS, W)
+            for side in (1, 0):
+                product = jnp.dot(cots_t[side, m], split, preferred_element_type=F32)
+                product = product[:, :RANK] + product[:, RANK:]
+                pieces[side, m] = product.T.reshape(FS, RS, W)
+                if side == 1:
+                    to_partner(pieces.at[1, m], from_core.at[m], m).start()
 
     def send_pieces(m):
         with jax.named_scope("wait_core"):
@@ -368,29 +391,39 @@
         squares.append(direction[:8] * direction[:8] + direction[8:] * direction[8:])
 
     loaded(0, fbuf.at[me])
-    groups = ring.steps(factor_arrived)
-
-    def to(group):
-        while next(groups) != group:
-            pass
-
-    to("start")
+
+    @pl.when(core == 1)
+    def _():
+        next(groups)
+
+    with jax.named_scope("turn"):
+        loaded(1, cots)
+        for m in range(3):
+
+            def turn(i, _):
+                rows = pl.ds(pl.multiple_of(i * 256, 256), 256)
+                cots_t[0, m, :, rows] = cots[m, rows, :].T
+                return _
+
+            lax.fori_loop(0, TOK // 256, turn, 0)
+
     to_partner(cots_t.at[0], cots_t.at[1], 3).start()
     with jax.named_scope("wait_loads"):
         loaded(2, left.at[0])
         loaded(3, left.at[1])
     multiply(me, first=True)
-    for group in ("2", "4_0", "4_-1", "4_2"):
-        to(group)
-        multiply(*waiting)
-        waiting.clear()
+    for group in ("3_0", "3_1", "3_2", "4_1"):
+        multiply(*slots_until(group))
     to_partner(cots_t.at[0], cots_t.at[1], 3).wait_recv()
+    last = slots_until("4_2")
     order = (odd_base, odd_base + 1, lacking)
+    multiply(*last, matrices=order[:1])
     project(order[0])
+    multiply(*last, matrices=order[1:2])
+    send_pieces(order[0])
     project(order[1])
-    send_pieces(order[0])
     with jax.named_scope("wait_y"):
-        along_y(fbuf.at[others, 0], 0).wait_recv()
+        along_y(fbuf.at[others, 0, pl.ds(0, HALF)], 0).wait_recv()
     multiply_lacking()
     send_pieces(order[1])
     project(order[2])
@@ -424,16 +457,15 @@
         if m == 2:
             upper, lower = high_low(full.T)
             contract = (((1,), (1,)), ((), ()))
-            own = fown[m]
+            own = fbuf[me, m]
             product = lax.dot_general(upper, own, contract, preferred_element_type=F32)
             product += lax.dot_general(lower, own, contract, preferred_element_type=F32)
         else:
             upper, lower = high_low(full)
-            product = jnp.dot(fown[m], upper, preferred_element_type=F32)
-            product += jnp.dot(fown[m], lower, preferred_element_type=F32)
+            product = jnp.dot(fbuf[me, m], upper, preferred_element_type=F32)
+            product += jnp.dot(fbuf[me, m], lower, preferred_element_type=F32)
         upd[m] = product
 
-    loaded(6, fown)
     loaded(5, wbuf)
     wait_directions(order[0])
     with jax.named_scope("wait_scalar"):
@@ -447,11 +479,31 @@
     loop(1, FS, send_sum)
     wait_directions(order[1])
     update(1)
-    ring.finish(fbuf.at[others, pl.ds(0, 2)])
-    along_y(fbuf.at[others, 0], 0).wait_send()
+
+    @pl.when(odd == 1)
+    def _():
+        update(0)
+
+    @pl.when(odd == 0)
+    def _():
+        update(2)
+
+    @pl.when(core == 1)
+    def _():
+        ring.finish(fbuf.at[others, pl.ds(0, 2)])
+        along_y(fbuf.at[others, 0], 0).wait_send()
+        to_other_core(fbuf.at[others, pl.ds(0, 2), pl.ds(0, HALF)], 0).wait_send()
+
     wait_directions(order[2])
-    update(0)
-    update(2)
+
+    @pl.when(odd == 0)
+    def _():
+        update(0)
+
+    @pl.when(odd == 1)
+    def _():
+        update(2)
+
     with jax.named_scope("wait_fs_scalar"):
         ref = fs_sums.at[others]
         to_fs(ref, ref, s_send.at[1], s_recv.at[1], 1).wait_recv()
@@ -537,8 +589,7 @@
             pltpu.VMEM((2, TOK, D // 2), BF16),
             pltpu.VMEM((3, TOK, W), BF16),
             pltpu.VMEM((2, 3, W, TOK), BF16),
-            pltpu.VMEM((FS, 3, HALF, RANK), BF16),
-            pltpu.VMEM((3, W, RANK), BF16),
+            pltpu.VMEM((FS, 3, W, RANK), BF16),
             pltpu.VMEM((3, W, W), F32),
             pltpu.VMEM((3, TOK, RANK), F32),
             pltpu.VMEM((2, 3, FS, RS, W), F32),
@@ -547,10 +598,11 @@
             pltpu.VMEM((3, FS, RS, W), F32),
             pltpu.VMEM((TP, 8, 128), F32),
             pltpu.VMEM((FS, 8, 128), F32),
-            dma((7,)),
+            dma((6,)),
             dma((1,)),
             dma((len(RECEIVED),)),
-            dma((2,)),
+            dma((3,)),
+            dma((5,)),
             dma((5,)),
             dma((1,)),
             dma((3,)),

time: 87.1 us -> 86.3 us (level)
  Pallas kernels: 86.4 us -> 85.2 us
    pallas_call x1, Pallas kernels: 83.5 us -> 82.3 us  [shards(): pl.pallas_call(kernel, out_shape=(pltpu.VMEM((2, 3, RS, W), F32), pltpu.V...]
where the time goes in v5:
time: 86.3 us; the launch traced here: 85.8 us
  Pallas kernels  85.2 us (99%)
    pallas_call x1, Pallas kernels, shards(): pl.pallas_call(kernel, out_shape=(pltpu.VMEM((2, 3, RS, W), F32), pltpu.V...  82.3 us
    pallas_call x1, Pallas kernels, shards(): pl.pallas_call(store_kernel, out_shape=(jax.ShapeDtypeStruct((3, RS, W),...  2.87 us

profile of v5, /device:TPU:0, one launch (start us, length us, event | category | flops | bytes accessed | tf_op | source)
XLA Modules:
  0.0 85.8 jit_solution(12191278089225934124)
XLA Ops:
  0.6 82.3 %shard_map.170 = (f32[2,3,16,256]{3,2,1,0:T(8,128)S(1)}, f32[3,256,256]{2,1,0:T(8,128)S(1)}, bf16[16,3,256,256]{3,2,1,0:T(8,128)(2,1)S(1)}) custom-call(bf16[1024,4096]{1,0:T(8,128)(2,1)} %inputs.1, bf16[1024,256]{1,0:T(8,128)(2,1)} %value_cot.1, bf16[1024,256]{1,0:T(8,128)(2,1)} %gate_cot.1, bf16[1024,4096]{1,0:T(8,128)(2,1)} %out_cot.1, ...), custom_call_target="tpu_custom_call" | custom-call | tf_op jit(solution)/shard_map/pallas_call | solution.py:579
  83.0 2.9 %shard_map.171 = (f32[3,16,256]{2,1,0:T(8,128)}, f32[3,16,256]{2,1,0:T(8,128)}, f32[256,256]{1,0:T(8,128)}, f32[256,256]{1,0:T(8,128)}, f32[256,256]{1,0:T(8,128...) custom-call(f32[2,3,16,256]{3,2,1,0:T(8,128)S(1)} %get-tuple-element.11.mom, ...), custom_call_target="tpu_custom_call" | custom-call | tf_op jit(solution)/shard_map/pallas_call | solution.py:618

commit v6 on v5

--- a/solution.py
+++ b/solution.py
@@ -173,6 +173,23 @@
     core = lax.rem(t, 2)
     partner = t + 1 - 2 * core
 
+    barrier = pltpu.get_barrier_semaphore()
+
+    def greet_fs(j, _):
+        pl.semaphore_signal(
+            barrier, inc=1, device_id={"fs": lax.rem(me + j, FS)}, device_id_type=MESH
+        )
+        return _
+
+    def greet_tp(j, _):
+        pl.semaphore_signal(
+            barrier, inc=1, device_id={"tp": lax.rem(t + j, TP)}, device_id_type=MESH
+        )
+        return _
+
+    lax.fori_loop(1, FS, greet_fs, 0)
+    lax.fori_loop(1, TP, greet_tp, 0)
+
     def load(at, *pairs):
         for src, dst in pairs:
             pltpu.make_async_copy(src, dst, load_sem.at[at]).start()
@@ -194,23 +211,6 @@
     lax.fori_loop(0, FS, load_half, 0)
     load(4, (first_moment, mom.at[0]), (second_moment, mom.at[1]))
     load(5, *((r, wbuf.at[m]) for m, r in enumerate((value_weight, gate_weight, out_weight))))
-
-    barrier = pltpu.get_barrier_semaphore()
-
-    def greet_fs(j, _):
-        pl.semaphore_signal(
-            barrier, inc=1, device_id={"fs": lax.rem(me + j, FS)}, device_id_type=MESH
-        )
-        return _
-
-    def greet_tp(j, _):
-        pl.semaphore_signal(
-            barrier, inc=1, device_id={"tp": lax.rem(t + j, TP)}, device_id_type=MESH
-        )
-        return _
-
-    lax.fori_loop(1, FS, greet_fs, 0)
-    lax.fori_loop(1, TP, greet_tp, 0)
 
     with jax.named_scope("barrier"):
         pl.semaphore_wait(barrier, FS - 1 + TP - 1)
@@ -314,12 +314,12 @@
             right = fbuf[:, lacking, half, :].reshape(D // 2, RANK)
 
             def tile(i, carry):
-                rows = pl.ds(pl.multiple_of(i * 256, 256), 256)
+                rows = pl.ds(pl.multiple_of(i * 512, 512), 512)
                 ours = left[lacking // 2, rows, :]
                 summed[lacking, rows, :] = jnp.dot(ours, right, preferred_element_type=F32)
                 return carry
 
-            lax.fori_loop(0, TOK // 256, tile, 0)
+            lax.fori_loop(0, TOK // 512, tile, 0)
 
     def loop(start, stop, step):
         def body(j, carry):
@@ -367,6 +367,16 @@
         loop(1, FS, send_piece)
         arrived[m, me] = pieces[0, m, me]
 
+    def to_tp(ref, j):
+        return pltpu.make_async_remote_copy(
+            src_ref=ref,
+            dst_ref=ref,
+            send_sem=s_send.at[0],
+            recv_sem=s_recv.at[0],
+            device_id={"tp": lax.rem(t + j, TP)},
+            device_id_type=MESH,
+        )
+
     squares = []
 
     def moments(m):
@@ -382,13 +392,17 @@
         mom[0, m] = new_first
         mom[1, m] = new_second
         dirs[m, me] = direction
+        squares.append(jnp.sum(direction * direction, axis=0, keepdims=True))
+        if len(squares) == 3:
+            square = squares[0] + squares[1] + squares[2]
+            sums[t] = square[:, :128] + square[:, 128:]
+            loop(1, TP, lambda j: to_tp(sums.at[t], j).start())
 
         def send_direction(j):
             ref = dirs.at[m, me]
             to_fs(ref, ref, d_send.at[0], d_recv.at[m], j).start()
 
         loop(1, FS, send_direction)
-        squares.append(direction[:8] * direction[:8] + direction[8:] * direction[8:])
 
     loaded(0, fbuf.at[me])
 
@@ -422,30 +436,15 @@
     multiply(*last, matrices=order[1:2])
     send_pieces(order[0])
     project(order[1])
+    send_pieces(order[1])
     with jax.named_scope("wait_y"):
         along_y(fbuf.at[others, 0, pl.ds(0, HALF)], 0).wait_recv()
     multiply_lacking()
-    send_pieces(order[1])
     project(order[2])
     send_pieces(order[2])
     loaded(4, mom)
     for m in order:
         moments(m)
-
-    square = squares[0] + squares[1] + squares[2]
-    sums[t] = square[:, :128] + square[:, 128:]
-
-    def to_tp(ref, j):
-        return pltpu.make_async_remote_copy(
-            src_ref=ref,
-            dst_ref=ref,
-            send_sem=s_send.at[0],
-            recv_sem=s_recv.at[0],
-            device_id={"tp": lax.rem(t + j, TP)},
-            device_id_type=MESH,
-        )
-
-    loop(1, TP, lambda j: to_tp(sums.at[t], j).start())
 
     def wait_directions(m):
         with jax.named_scope("wait_directions"):
@@ -596,8 +595,8 @@
             pltpu.VMEM((3, FS, RS, W), F32),
             pltpu.VMEM((3, FS, RS, W), F32),
             pltpu.VMEM((3, FS, RS, W), F32),
-            pltpu.VMEM((TP, 8, 128), F32),
-            pltpu.VMEM((FS, 8, 128), F32),
+            pltpu.VMEM((TP, 1, 128), F32),
+            pltpu.VMEM((FS, 1, 128), F32),
             dma((6,)),
             dma((1,)),
             dma((len(RECEIVED),)),

time: 86.3 us -> 84.9 us (0.984)
  Pallas kernels: 85.2 us -> 83.9 us
    pallas_call x1, Pallas kernels: 82.3 us -> 81.1 us  [shards(): pl.pallas_call(kernel, out_shape=(pltpu.VMEM((2, 3, RS, W), F32), pltpu.V...]
where the time goes in v6:
time: 84.9 us; the launch traced here: 84.6 us
  Pallas kernels  83.9 us (99%)
    pallas_call x1, Pallas kernels, shards(): pl.pallas_call(kernel, out_shape=(pltpu.VMEM((2, 3, RS, W), F32), pltpu.V...  81.1 us
    pallas_call x1, Pallas kernels, shards(): pl.pallas_call(store_kernel, out_shape=(jax.ShapeDtypeStruct((3, RS, W),...  2.87 us

profile of v6, /device:TPU:0, one launch (start us, length us, event | category | flops | bytes accessed | tf_op | source)
XLA Modules:
  0.0 84.6 jit_solution(10093594175293421902)
XLA Ops:
  0.6 81.1 %shard_map.170 = (f32[2,3,16,256]{3,2,1,0:T(8,128)S(1)}, f32[3,256,256]{2,1,0:T(8,128)S(1)}, bf16[16,3,256,256]{3,2,1,0:T(8,128)(2,1)S(1)}) custom-call(bf16[1024,4096]{1,0:T(8,128)(2,1)} %inputs.1, bf16[1024,256]{1,0:T(8,128)(2,1)} %value_cot.1, bf16[1024,256]{1,0:T(8,128)(2,1)} %gate_cot.1, bf16[1024,4096]{1,0:T(8,128)(2,1)} %out_cot.1, ...), custom_call_target="tpu_custom_call" | custom-call | tf_op jit(solution)/shard_map/pallas_call | solution.py:578
  81.7 2.9 %shard_map.171 = (f32[3,16,256]{2,1,0:T(8,128)}, f32[3,16,256]{2,1,0:T(8,128)}, f32[256,256]{1,0:T(8,128)}, f32[256,256]{1,0:T(8,128)}, f32[256,256]{1,0:T(8,128...) custom-call(f32[2,3,16,256]{3,2,1,0:T(8,128)S(1)} %get-tuple-element.11.mom, ...), custom_call_target="tpu_custom_call" | custom-call | tf_op jit(solution)/shard_map/pallas_call | solution.py:617

commit v7 on v6

--- a/solution.py
+++ b/solution.py
@@ -36,7 +36,8 @@
 
 
 class RingGather:
-    def __init__(self, name, me, part, send, recv):
+    def __init__(self, name, me, part, send, recv, near=None):
+        self.near = near
         self.name = name
         self.z, self.x = me // SIDE, lax.rem(me, SIDE)
         self.part, self.send, self.recv = part, send, recv
@@ -58,17 +59,22 @@
             device_id_type=MESH,
         )
 
+    def ref(self, k, stage, po, s, half):
+        if self.near and k == 0 and (stage == 1 or (stage == 3 and po == 0)):
+            return self.near(s)
+        return self.part(s, k, half)
+
     def start(self, k, stage, po, d):
         first = stage in (1, 2)
         at = {1: (0, 0), 2: (-d, 0), 3: (po, 0), 4: (po, -d)}[stage]
         half = None if stage in (1, 3) else (0 if d > 0 else 1)
         to = self.slot(k, d, 0) if first else self.slot(k, 0, d)
-        ref = self.part(self.slot(k, *at), k, half)
+        ref = self.ref(k, stage, po, self.slot(k, *at), half)
         self.copy(ref, k, stage, po, d, to).start()
 
     def wait(self, k, stage, po, d=0):
         at = {1: (-d, 0), 2: (2, 0), 3: (po, -d), 4: (po, 2)}[stage]
-        ref = self.part(self.slot(k, *at), k, None)
+        ref = self.ref(k, stage, po, self.slot(k, *at), None)
         with jax.named_scope(f"w{self.name}_{k}_{stage}_{po}_{d}"):
             self.copy(ref, k, stage, po, d, self.slot(k, 1, 0)).wait_recv()
 
@@ -148,6 +154,7 @@
     cots_t,
     fbuf,
     wbuf,
+    near_w,
     summed,
     pieces,
     from_core,
@@ -167,6 +174,8 @@
     d_recv,
     s_send,
     s_recv,
+    w_send,
+    w_recv,
 ):
     me = lax.axis_index("fs")
     t = lax.axis_index("tp")
@@ -426,8 +435,36 @@
         loaded(2, left.at[0])
         loaded(3, left.at[1])
     multiply(me, first=True)
+    near_slots = [ring.slot(0, *at) for at in ((-1, 0), (1, 0), (0, -1), (0, 1))]
+
+    def weights_to(i):
+        at = ((1, 0), (-1, 0), (0, 1), (0, -1))[i]
+        return pltpu.make_async_remote_copy(
+            src_ref=wbuf.at[pl.ds(0, 2), half, :],
+            dst_ref=near_w.at[i],
+            send_sem=w_send.at[0],
+            recv_sem=w_recv.at[0],
+            device_id={"fs": ring.slot(0, *at)},
+            device_id_type=MESH,
+        )
+
+    def all_weights():
+        return pltpu.make_async_remote_copy(
+            src_ref=near_w,
+            dst_ref=near_w,
+            send_sem=w_send.at[0],
+            recv_sem=w_recv.at[0],
+            device_id={"fs": near_slots[0]},
+            device_id_type=MESH,
+        )
+
     for group in ("3_0", "3_1", "3_2", "4_1"):
-        multiply(*slots_until(group))
+        slots = slots_until(group)
+        if group == "3_2":
+            loaded(5, wbuf)
+            for i in range(4):
+                weights_to(i).start()
+        multiply(*slots)
     to_partner(cots_t.at[0], cots_t.at[1], 3).wait_recv()
     last = slots_until("4_2")
     order = (odd_base, odd_base + 1, lacking)
@@ -465,7 +502,6 @@
             product += jnp.dot(fbuf[me, m], lower, preferred_element_type=F32)
         upd[m] = product
 
-    loaded(5, wbuf)
     wait_directions(order[0])
     with jax.named_scope("wait_scalar"):
         to_tp(sums.at[pl.ds(0, TP - 1)], 1).wait_recv()
@@ -513,18 +549,38 @@
         upd[m] = scaled
         copies[me, m] = (wbuf[m] - LEARN_RATE * scaled).astype(BF16)
 
-    def copy_part(s, k, half):
-        at, size = 128 * k, 128
-        if half is not None:
-            at, size = at + 64 * half, 64
-        return copies.at[s, :, pl.ds(at, size), :]
-
-    gather = RingGather("c", me, copy_part, ring_send.at[0], ring_recv)
-    for _ in gather.steps(lambda k, po, qo: None):
-        pass
+    def copy_part(s, k, part_half):
+        at, size = HALF * (k + core - 2 * k * core), HALF
+        if part_half is not None:
+            at, size = at + 64 * part_half, 64
+        return copies.at[s, :, pl.ds(pl.multiple_of(at, 64), size), :]
+
+    def copy_near(s):
+        return copies.at[s, pl.ds(2, 1), half, :]
+
+    def near_copies():
+        with jax.named_scope("wait_near"):
+            all_weights().wait_recv()
+        with jax.named_scope("near"):
+            for m in range(2):
+                upper, lower = high_low(dirs[m].reshape(RANK, W))
+                rows = jnp.concatenate([fbuf[s, m, half, :] for s in near_slots], axis=0)
+                product = jnp.dot(rows, upper, preferred_element_type=F32)
+                product += jnp.dot(rows, lower, preferred_element_type=F32)
+                scaled = norm_scale * product
+                for i, s in enumerate(near_slots):
+                    update = scaled[HALF * i : HALF * (i + 1)]
+                    copies[s, m, half, :] = (near_w[i, m] - LEARN_RATE * update).astype(BF16)
+
+    gather = RingGather("c", me, copy_part, ring_send.at[0], ring_recv, copy_near)
+    for group in gather.steps(lambda k, po, qo: None):
+        if group == "start":
+            near_copies()
 
     with jax.named_scope("finish"):
-        gather.finish(copies.at[others])
+        gather.finish(copies.at[pl.ds(0, 13)])
+        gather.finish(copies.at[pl.ds(0, 4), 0, pl.ds(0, HALF)])
+        all_weights().wait_send()
         to_partner(cots_t.at[0], cots_t.at[1], 3).wait_send()
         for m in range(3):
             to_partner(pieces.at[1, m], from_core.at[m], m).wait_send()
@@ -590,6 +646,7 @@
             pltpu.VMEM((2, 3, W, TOK), BF16),
             pltpu.VMEM((FS, 3, W, RANK), BF16),
             pltpu.VMEM((3, W, W), F32),
+            pltpu.VMEM((4, 2, HALF, W), F32),
             pltpu.VMEM((3, TOK, RANK), F32),
             pltpu.VMEM((2, 3, FS, RS, W), F32),
             pltpu.VMEM((3, FS, RS, W), F32),
@@ -609,6 +666,8 @@
             dma((3,)),
             dma((2,)),
             dma((2,)),
+            dma((1,)),
+            dma((1,)),
         ],
         compiler_params=pltpu.CompilerParams(
             collective_id=0, has_side_effects=True, vmem_limit_bytes=48 * 1024 * 1024

time: 84.9 us -> 82.2 us (0.968)
  Pallas kernels: 83.9 us -> 81.2 us
    pallas_call x1, Pallas kernels: 81.1 us -> 78.3 us  [shards(): pl.pallas_call(kernel, out_shape=(pltpu.VMEM((2, 3, RS, W), F32), pltpu.V...]
where the time goes in v7:
time: 82.2 us; the launch traced here: 81.8 us
  Pallas kernels  81.2 us (99%)
    pallas_call x1, Pallas kernels, shards(): pl.pallas_call(kernel, out_shape=(pltpu.VMEM((2, 3, RS, W), F32), pltpu.V...  78.3 us
    pallas_call x1, Pallas kernels, shards(): pl.pallas_call(store_kernel, out_shape=(jax.ShapeDtypeStruct((3, RS, W),...  2.87 us

profile of v7, /device:TPU:0, one launch (start us, length us, event | category | flops | bytes accessed | tf_op | source)
XLA Modules:
  0.0 81.8 jit_solution(17354266221379538896)
XLA Ops:
  0.6 78.3 %shard_map.170 = (f32[2,3,16,256]{3,2,1,0:T(8,128)S(1)}, f32[3,256,256]{2,1,0:T(8,128)S(1)}, bf16[16,3,256,256]{3,2,1,0:T(8,128)(2,1)S(1)}) custom-call(bf16[1024,4096]{1,0:T(8,128)(2,1)} %inputs.1, bf16[1024,256]{1,0:T(8,128)(2,1)} %value_cot.1, bf16[1024,256]{1,0:T(8,128)(2,1)} %gate_cot.1, bf16[1024,4096]{1,0:T(8,128)(2,1)} %out_cot.1, ...), custom_call_target="tpu_custom_call" | custom-call | tf_op jit(solution)/shard_map/pallas_call | solution.py:634
  78.9 2.9 %shard_map.171 = (f32[3,16,256]{2,1,0:T(8,128)}, f32[3,16,256]{2,1,0:T(8,128)}, f32[256,256]{1,0:T(8,128)}, f32[256,256]{1,0:T(8,128)}, f32[256,256]{1,0:T(8,128...) custom-call(f32[2,3,16,256]{3,2,1,0:T(8,128)S(1)} %get-tuple-element.11.mom, ...), custom_call_target="tpu_custom_call" | custom-call | tf_op jit(solution)/shard_map/pallas_call | solution.py:676

commit v8 on v7

--- a/solution.py
+++ b/solution.py
@@ -36,7 +36,7 @@
 
 
 class RingGather:
-    def __init__(self, name, me, part, send, recv, near=None):
+    def __init__(self, name, me, part, send, recv, near=False):
         self.near = near
         self.name = name
         self.z, self.x = me // SIDE, lax.rem(me, SIDE)
@@ -59,22 +59,22 @@
             device_id_type=MESH,
         )
 
-    def ref(self, k, stage, po, s, half):
-        if self.near and k == 0 and (stage == 1 or (stage == 3 and po == 0)):
-            return self.near(s)
-        return self.part(s, k, half)
+    def skipped(self, k, stage, po):
+        return self.near and k == 0 and (stage == 1 or (stage == 3 and po == 0))
 
     def start(self, k, stage, po, d):
         first = stage in (1, 2)
         at = {1: (0, 0), 2: (-d, 0), 3: (po, 0), 4: (po, -d)}[stage]
         half = None if stage in (1, 3) else (0 if d > 0 else 1)
         to = self.slot(k, d, 0) if first else self.slot(k, 0, d)
-        ref = self.ref(k, stage, po, self.slot(k, *at), half)
+        if self.skipped(k, stage, po):
+            return
+        ref = self.part(self.slot(k, *at), k, half)
         self.copy(ref, k, stage, po, d, to).start()
 
     def wait(self, k, stage, po, d=0):
         at = {1: (-d, 0), 2: (2, 0), 3: (po, -d), 4: (po, 2)}[stage]
-        ref = self.ref(k, stage, po, self.slot(k, *at), None)
+        ref = self.part(self.slot(k, *at), k, None)
         with jax.named_scope(f"w{self.name}_{k}_{stage}_{po}_{d}"):
             self.copy(ref, k, stage, po, d, self.slot(k, 1, 0)).wait_recv()
 
@@ -84,8 +84,12 @@
                 for k in (0, 1):
                     self.start(k, stage, 0, d)
         yield "start"
+        if self.near:
+            for d in (1, -1):
+                self.start(0, 2, 0, d)
+                self.start(0, 4, 0, d)
         for d in (1, -1):
-            for k in (0, 1):
+            for k in (1,) if self.near else (0, 1):
                 self.wait(k, 1, 0, d)
                 self.start(k, 2, 0, d)
                 arrived(k, -d, 0)
@@ -116,8 +120,9 @@
     def second(self, arrived, po):
         for d in (1, -1):
             for k in (0, 1):
-                self.wait(k, 3, po, d)
-                self.start(k, 4, po, d)
+                if not self.skipped(k, 3, po):
+                    self.wait(k, 3, po, d)
+                    self.start(k, 4, po, d)
                 arrived(k, po, -d)
 
     def last(self, arrived, po):
@@ -155,6 +160,9 @@
     fbuf,
     wbuf,
     near_w,
+    near_out,
+    near_f,
+    turned,
     summed,
     pieces,
     from_core,
@@ -437,24 +445,14 @@
     multiply(me, first=True)
     near_slots = [ring.slot(0, *at) for at in ((-1, 0), (1, 0), (0, -1), (0, 1))]
 
-    def weights_to(i):
-        at = ((1, 0), (-1, 0), (0, 1), (0, -1))[i]
-        return pltpu.make_async_remote_copy(
-            src_ref=wbuf.at[pl.ds(0, 2), half, :],
-            dst_ref=near_w.at[i],
-            send_sem=w_send.at[0],
-            recv_sem=w_recv.at[0],
-            device_id={"fs": ring.slot(0, *at)},
-            device_id_type=MESH,
-        )
-
-    def all_weights():
-        return pltpu.make_async_remote_copy(
-            src_ref=near_w,
-            dst_ref=near_w,
-            send_sem=w_send.at[0],
-            recv_sem=w_recv.at[0],
-            device_id={"fs": near_slots[0]},
+    def weights_to(i, src, dst, at):
+        to = ((1, 0), (-1, 0), (0, 1), (0, -1))[i]
+        return pltpu.make_async_remote_copy(
+            src_ref=src,
+            dst_ref=dst,
+            send_sem=w_send.at[at],
+            recv_sem=w_recv.at[at],
+            device_id={"fs": ring.slot(0, *to)},
             device_id_type=MESH,
         )
 
@@ -463,7 +461,7 @@
         if group == "3_2":
             loaded(5, wbuf)
             for i in range(4):
-                weights_to(i).start()
+                weights_to(i, wbuf.at[pl.ds(0, 2), half, :], near_w.at[i], 0).start()
         multiply(*slots)
     to_partner(cots_t.at[0], cots_t.at[1], 3).wait_recv()
     last = slots_until("4_2")
@@ -476,6 +474,29 @@
     send_pieces(order[1])
     with jax.named_scope("wait_y"):
         along_y(fbuf.at[others, 0, pl.ds(0, HALF)], 0).wait_recv()
+
+    def near_factor(i):
+        return pltpu.make_async_remote_copy(
+            src_ref=fbuf.at[near_slots[i], 2, half, :],
+            dst_ref=near_f.at[i],
+            send_sem=w_send.at[1],
+            recv_sem=w_recv.at[1],
+            device_id={"tp": partner},
+            device_id_type=MESH,
+        )
+
+    def near_factors():
+        return pltpu.make_async_remote_copy(
+            src_ref=near_f,
+            dst_ref=near_f,
+            send_sem=w_send.at[1],
+            recv_sem=w_recv.at[1],
+            device_id={"tp": partner},
+            device_id_type=MESH,
+        )
+
+    for i in range(4):
+        near_factor(i).start()
     multiply_lacking()
     project(order[2])
     send_pieces(order[2])
@@ -512,6 +533,8 @@
         to_fs(ref, ref, s_send.at[1], s_recv.at[1], j).start()
 
     loop(1, FS, send_sum)
+    for i in range(4):
+        weights_to(i, wbuf.at[2, half, :], near_out.at[i], 2).start()
     wait_directions(order[1])
     update(1)
 
@@ -555,12 +578,10 @@
             at, size = at + 64 * part_half, 64
         return copies.at[s, :, pl.ds(pl.multiple_of(at, 64), size), :]
 
-    def copy_near(s):
-        return copies.at[s, pl.ds(2, 1), half, :]
-
     def near_copies():
         with jax.named_scope("wait_near"):
-            all_weights().wait_recv()
+            weights_to(0, near_w, near_w, 0).wait_recv()
+            near_factors().wait_recv()
         with jax.named_scope("near"):
             for m in range(2):
                 upper, lower = high_low(dirs[m].reshape(RANK, W))
@@ -571,16 +592,37 @@
                 for i, s in enumerate(near_slots):
                     update = scaled[HALF * i : HALF * (i + 1)]
                     copies[s, m, half, :] = (near_w[i, m] - LEARN_RATE * update).astype(BF16)
-
-    gather = RingGather("c", me, copy_part, ring_send.at[0], ring_recv, copy_near)
+        with jax.named_scope("wait_near_out"):
+            weights_to(0, near_out, near_out, 2).wait_recv()
+        with jax.named_scope("near_out"):
+            turned[...] = dirs[2].reshape(RANK, W).T
+            upper, lower = high_low(turned[half, :])
+            contract = (((1,), (1,)), ((), ()))
+            other_half = pl.ds(pl.multiple_of((1 - core) * HALF, HALF), HALF)
+            for cols, rows in (
+                (half, [fbuf[s, 2, half, :] for s in near_slots]),
+                (other_half, [near_f[i] for i in range(4)]),
+            ):
+                rows = jnp.concatenate(rows, axis=0)
+                product = lax.dot_general(upper, rows, contract, preferred_element_type=F32)
+                product += lax.dot_general(lower, rows, contract, preferred_element_type=F32)
+                scaled = norm_scale * product
+                for i, s in enumerate(near_slots):
+                    update = scaled[:, HALF * i : HALF * (i + 1)]
+                    copies[s, 2, half, cols] = (
+                        near_out[i, :, cols] - LEARN_RATE * update
+                    ).astype(BF16)
+
+    gather = RingGather("c", me, copy_part, ring_send.at[0], ring_recv, True)
     for group in gather.steps(lambda k, po, qo: None):
         if group == "start":
             near_copies()
 
     with jax.named_scope("finish"):
         gather.finish(copies.at[pl.ds(0, 13)])
-        gather.finish(copies.at[pl.ds(0, 4), 0, pl.ds(0, HALF)])
-        all_weights().wait_send()
+        weights_to(0, near_w, near_w, 0).wait_send()
+        near_factors().wait_send()
+        weights_to(0, near_out, near_out, 2).wait_send()
         to_partner(cots_t.at[0], cots_t.at[1], 3).wait_send()
         for m in range(3):
             to_partner(pieces.at[1, m], from_core.at[m], m).wait_send()
@@ -647,6 +689,9 @@
             pltpu.VMEM((FS, 3, W, RANK), BF16),
             pltpu.VMEM((3, W, W), F32),
             pltpu.VMEM((4, 2, HALF, W), F32),
+            pltpu.VMEM((4, HALF, W), F32),
+            pltpu.VMEM((4, HALF, RANK), BF16),
+            pltpu.VMEM((W, RANK), F32),
             pltpu.VMEM((3, TOK, RANK), F32),
             pltpu.VMEM((2, 3, FS, RS, W), F32),
             pltpu.VMEM((3, FS, RS, W), F32),
@@ -666,8 +711,8 @@
             dma((3,)),
             dma((2,)),
             dma((2,)),
-            dma((1,)),
-            dma((1,)),
+            dma((3,)),
+            dma((3,)),
         ],
         compiler_params=pltpu.CompilerParams(
             collective_id=0, has_side_effects=True, vmem_limit_bytes=48 * 1024 * 1024

time: 82.2 us -> 80.7 us (0.982)
  Pallas kernels: 81.2 us -> 79.9 us
    pallas_call x1, Pallas kernels: 78.3 us -> 77 us  [shards(): pl.pallas_call(kernel, out_shape=(pltpu.VMEM((2, 3, RS, W), F32), pltpu.V...]
where the time goes in v8:
time: 80.7 us; the launch traced here: 80.6 us
  Pallas kernels  79.9 us (99%)
    pallas_call x1, Pallas kernels, shards(): pl.pallas_call(kernel, out_shape=(pltpu.VMEM((2, 3, RS, W), F32), pltpu.V...  77 us
    pallas_call x1, Pallas kernels, shards(): pl.pallas_call(store_kernel, out_shape=(jax.ShapeDtypeStruct((3, RS, W),...  2.87 us

profile of v8, /device:TPU:0, one launch (start us, length us, event | category | flops | bytes accessed | tf_op | source)
XLA Modules:
  0.0 80.6 jit_solution(11385063246100455)
XLA Ops:
  0.6 77.0 %shard_map.170 = (f32[2,3,16,256]{3,2,1,0:T(8,128)S(1)}, f32[3,256,256]{2,1,0:T(8,128)S(1)}, bf16[16,3,256,256]{3,2,1,0:T(8,128)(2,1)S(1)}) custom-call(bf16[1024,4096]{1,0:T(8,128)(2,1)} %inputs.1, bf16[1024,256]{1,0:T(8,128)(2,1)} %value_cot.1, bf16[1024,256]{1,0:T(8,128)(2,1)} %gate_cot.1, bf16[1024,4096]{1,0:T(8,128)(2,1)} %out_cot.1, ...), custom_call_target="tpu_custom_call" | custom-call | tf_op jit(solution)/shard_map/pallas_call | solution.py:676
  77.7 2.9 %shard_map.171 = (f32[3,16,256]{2,1,0:T(8,128)}, f32[3,16,256]{2,1,0:T(8,128)}, f32[256,256]{1,0:T(8,128)}, f32[256,256]{1,0:T(8,128)}, f32[256,256]{1,0:T(8,128...) custom-call(f32[2,3,16,256]{3,2,1,0:T(8,128)S(1)} %get-tuple-element.11.mom, ...), custom_call_target="tpu_custom_call" | custom-call | tf_op jit(solution)/shard_map/pallas_call | solution.py:721

commit v9 on v8

--- a/solution.py
+++ b/solution.py
@@ -106,23 +106,33 @@
             self.start(k, 3, 2, -1)
             arrived(k, 2, 0)
         yield "2"
-        for po in (-1, 1):
-            self.second(arrived, po)
-            yield f"3_{po}"
-        self.last(arrived, 0)
-        yield "4_0"
-        self.second(arrived, 2)
-        yield "3_2"
+        if self.near:
+            self.second(arrived, -1)
+            self.second(arrived, 1, later=True)
+            self.second(arrived, 2)
+            for k in (0, 1):
+                for d in (1, -1):
+                    self.start(k, 4, 1, d)
+            self.last(arrived, 0)
+        else:
+            for po in (-1, 1):
+                self.second(arrived, po)
+                yield f"3_{po}"
+            self.last(arrived, 0)
+            yield "4_0"
+            self.second(arrived, 2)
+            yield "3_2"
         for po in (-1, 1, 2):
             self.last(arrived, po)
             yield f"4_{po}"
 
-    def second(self, arrived, po):
+    def second(self, arrived, po, later=False):
         for d in (1, -1):
             for k in (0, 1):
                 if not self.skipped(k, 3, po):
                     self.wait(k, 3, po, d)
-                    self.start(k, 4, po, d)
+                    if not later:
+                        self.start(k, 4, po, d)
                 arrived(k, po, -d)
 
     def last(self, arrived, po):

time: 80.7 us -> 80.7 us (level)
  no operation moved by 1% of the time
where the time goes in v9:
time: 80.7 us; the launch traced here: 80.6 us
  Pallas kernels  79.9 us (99%)
    pallas_call x1, Pallas kernels, shards(): pl.pallas_call(kernel, out_shape=(pltpu.VMEM((2, 3, RS, W), F32), pltpu.V...  77.1 us
    pallas_call x1, Pallas kernels, shards(): pl.pallas_call(store_kernel, out_shape=(jax.ShapeDtypeStruct((3, RS, W),...  2.87 us

profile of v9, /device:TPU:0, one launch (start us, length us, event | category | flops | bytes accessed | tf_op | source)
XLA Modules:
  0.0 80.6 jit_solution(8583458838279766465)
XLA Ops:
  0.6 77.1 %shard_map.170 = (f32[2,3,16,256]{3,2,1,0:T(8,128)S(1)}, f32[3,256,256]{2,1,0:T(8,128)S(1)}, bf16[16,3,256,256]{3,2,1,0:T(8,128)(2,1)S(1)}) custom-call(bf16[1024,4096]{1,0:T(8,128)(2,1)} %inputs.1, bf16[1024,256]{1,0:T(8,128)(2,1)} %value_cot.1, bf16[1024,256]{1,0:T(8,128)(2,1)} %gate_cot.1, bf16[1024,4096]{1,0:T(8,128)(2,1)} %out_cot.1, ...), custom_call_target="tpu_custom_call" | custom-call | tf_op jit(solution)/shard_map/pallas_call | solution.py:686
  77.7 2.9 %shard_map.171 = (f32[3,16,256]{2,1,0:T(8,128)}, f32[3,16,256]{2,1,0:T(8,128)}, f32[256,256]{1,0:T(8,128)}, f32[256,256]{1,0:T(8,128)}, f32[256,256]{1,0:T(8,128...) custom-call(f32[2,3,16,256]{3,2,1,0:T(8,128)S(1)} %get-tuple-element.11.mom, ...), custom_call_target="tpu_custom_call" | custom-call | tf_op jit(solution)/shard_map/pallas_call | solution.py:731
